TPU v7x, 256 devices: a whole 4x4x8 slice. The times are simulated.
256 devices in a mesh: sp: 32 (over z, y), tp: 8 (over x, core).
Axes of the slice: x: 4, y: 4, z: 8, core: 2. Of those that a mesh axis runs over, the one named last changes fastest.
Arguments:
- head_value_rows: bfloat16 [24576, 2048], P('sp', 'tp'), may hold values from -6 to 6
- entry_map_rows: bfloat16 [24576, 1024], P('sp', 'tp'), may hold values from -6 to 6
- readout_map_rows: bfloat16 [24576, 1024], P('sp', 'tp'), may hold values from -6 to 6
- output_gate_rows: bfloat16 [24576, 2048], P('sp', 'tp'), may hold values from -6 to 6
- step_before_softplus: bfloat16 [24576, 32], P('sp', 'tp'), may hold values from -8 to 8
- sudden_log_decay: float32 [24576, 32], P('sp', 'tp'), may hold values from -1 to 0
- document_index: int32 [24576], replicated, may hold values from 0 to 7, never falling along the last dimension, each value on 1 to 6144 neighbouring positions
- head_rate_logarithm: float32 [2, 32], P(None, 'tp'), may hold values from -30 to 0
- head_step_bias: float32 [2, 32], P(None, 'tp'), may hold values from -3 to 3
- value_conv_taps: bfloat16 [5, 2048], P(None, 'tp'), may hold values from -2.5 to 2.5
- entry_conv_taps: bfloat16 [5, 1024], P(None, 'tp'), may hold values from -2.5 to 2.5
- readout_conv_taps: bfloat16 [5, 1024], P(None, 'tp'), may hold values from -2.5 to 2.5
- group_norm_gain: float32 [2048], P('tp'), may hold values from 0.1 to 1.9
- mixer_output_weight: bfloat16 [2048, 2048], P('tp'), may hold values from -0.125 to 0.125
- stream: bfloat16 [24576, 2048], P('sp', 'tp'), may hold values from -200 to 200
- mixer_norm_gain: float32 [2048], P('tp'), may hold values from 0.1 to 1.9
- channel_norm_gain: float32 [2048], P('tp'), may hold values from 0.1 to 1.9
- up_projection_weight: bfloat16 [2048, 8192], P('sp', 'tp'), may hold values from -0.125 to 0.125
- down_projection_weight: bfloat16 [2048, 8192], P('sp', 'tp'), may hold values from -0.0625 to 0.0625
Outputs:
- mixed: bfloat16 [24576, 2048], P('sp', 'tp')
All inputs are finite; a program needn't handle non-finite values.
Results may differ from a plain program's by a relative error of at most 0.018.
Values may be sent and summed in bfloat16 or wider, within the bound.
A program may use at most 64 MiB of HBM per device.

v0:
```python
import jax
import jax.numpy as jnp
from jax import lax
from jax.sharding import Mesh
from jax.sharding import PartitionSpec as P

D = 2048
HEAD_DIM = 64
STATE = 128
BLOCK = 128
SP = ("sp_0", "sp_1")


norm_eps = 1e-05
resid_scale = 1.4142135623730951


def padded(block, sides, width):
    for axis, dim in sides:
        count = lax.axis_size(axis)
        forward = [(i, i + 1) for i in range(count - 1)]
        backward = [(target, source) for source, target in forward]
        low = lax.ppermute(
            lax.slice_in_dim(block, block.shape[dim] - width, None, axis=dim), axis, forward
        )
        high = lax.ppermute(lax.slice_in_dim(block, 0, width, axis=dim), axis, backward)
        block = jnp.concatenate([low, block, high], axis=dim)
    return block


def nothing_yet(array, identity):
    return jax.tree.map(
        lambda a, e: jnp.broadcast_to(jnp.asarray(e, a.dtype), a.shape), array, identity
    )


def carried_in(array, axes, combine, identity, reverse):
    before = start = nothing_yet(array, identity)
    subtotal = array
    for axis in reversed(axes):
        count, index = (lax.axis_size(axis), lax.axis_index(axis))
        pieces = jax.tree.map(
            lambda part, kind: lax.all_gather(part.astype(kind), axis),
            subtotal,
            (jnp.bfloat16, jnp.bfloat16),
        )
        inside, subtotal = (start, start)
        for k in reversed(range(count)) if reverse else range(count):
            passed = k > index if reverse else k < index
            subtotal = combine(
                subtotal, jax.tree.map(lambda part, own: part[k].astype(own.dtype), pieces, array)
            )
            inside = jax.tree.map(lambda new, old: jnp.where(passed, new, old), subtotal, inside)
        before = combine(inside, before)
    return before


def cut_along(array, dim, count):
    dims = array.shape
    blocks = array.reshape(*dims[:dim], count, dims[dim] // count, *dims[dim + 1 :])
    return jnp.moveaxis(blocks, dim, 0)


def sent_and_summed(array, axis, dim):
    blocks = cut_along(array, dim, lax.axis_size(axis))
    arrived = lax.all_to_all(blocks, axis, split_axis=0, concat_axis=0, tiled=True)
    return arrived.astype(jnp.float32).sum(axis=0)


def block_step(running, blocks):
    states, last_doc = running
    scaled, entries, readout, decay_logarithm, block_ids = blocks
    block_len = block_ids.shape[0]
    cum_decay = jnp.cumsum(decay_logarithm, axis=0)
    indices = lax.iota(jnp.int32, block_len)
    linked = (indices[:, None] >= indices[None, :]) & (block_ids[:, None] == block_ids[None, :])
    link_mask = linked[:, :, None, None]
    spread = cum_decay[:, None] - cum_decay[None, :]
    weights = jnp.where(link_mask, jnp.exp(jnp.where(link_mask, spread, 0.0)), 0.0)
    scores = jnp.einsum("tgn,sgn->tsg", readout, entries)
    within = jnp.einsum("tsg,tsgr,sgrp->tgrp", scores, weights, scaled)
    arrival = jnp.where((block_ids == last_doc)[:, None, None], jnp.exp(cum_decay), 0.0)
    carried = jnp.einsum("tgn,grpn->tgrp", readout, states) * arrival[..., None]
    end_doc = block_ids[-1]
    to_end = jnp.where(
        (block_ids == end_doc)[:, None, None], jnp.exp(cum_decay[-1] - cum_decay), 0.0
    )
    passing = jnp.where(end_doc == last_doc, jnp.exp(cum_decay[-1]), 0.0)
    fresh = jnp.einsum("sgn,sgr,sgrp->grpn", entries, to_end, scaled)
    return ((states * passing[..., None, None] + fresh, end_doc), within + carried)


def sweep_blocks(
    scaled, entries, readout, decay_logarithm, document_index, states, last_doc, block_len
):
    row_count = document_index.shape[0]
    block_count = row_count // block_len

    def in_blocks(array):
        return array.reshape((block_count, block_len) + array.shape[1:])

    inputs = tuple(
        (in_blocks(array) for array in (scaled, entries, readout, decay_logarithm, document_index))
    )
    (states, last_doc), output = lax.scan(block_step, (states, last_doc), inputs)
    return (output.reshape((row_count,) + output.shape[2:]), states)


def chain(earlier, later):
    return (earlier[0] * later[0], earlier[1] * later[0][..., None, None] + later[1])


def norm_rows(residual, gain, width):
    sums = lax.psum((jnp.sum(residual, axis=1), jnp.sum(residual * residual, axis=1)), "tp")
    row_mean = sums[0] / width
    row_var = sums[1] / width - row_mean * row_mean
    return ((residual - row_mean[:, None]) * lax.rsqrt(row_var + norm_eps)[:, None] * gain).astype(
        jnp.bfloat16
    )


def per_device(
    head_value_rows,
    entry_map_rows,
    readout_map_rows,
    output_gate_rows,
    step_before_softplus,
    sudden_log_decay,
    document_index,
    head_rate_logarithm,
    head_step_bias,
    value_conv_taps,
    entry_conv_taps,
    readout_conv_taps,
    group_norm_gain,
    mixer_output_weight,
    stream,
    mixer_norm_gain,
    channel_norm_gain,
    up_projection_weight,
    down_projection_weight,
):
    row_count = head_value_rows.shape[0]
    head_count = step_before_softplus.shape[1]
    groups = entry_map_rows.shape[1] // STATE
    per_group = head_count // groups
    value_width = head_value_rows.shape[1]
    state_width = entry_map_rows.shape[1]
    joined = jnp.concatenate([head_value_rows, entry_map_rows, readout_map_rows], axis=1)
    conv_all = jnp.concatenate(
        [value_conv_taps, entry_conv_taps, readout_conv_taps], axis=1
    ).astype(jnp.float32)
    taps = conv_all.shape[0]
    half_width = taps // 2
    extended = padded(joined, ((SP, 0),), half_width).astype(jnp.float32)
    position = lax.axis_index(SP) * row_count
    doc_pad = jnp.pad(document_index, half_width + 1, constant_values=-1)
    window_ids = lax.dynamic_slice_in_dim(doc_pad, position + 1, row_count + 2 * half_width)
    own_ids = window_ids[half_width : half_width + row_count]
    prev_id = lax.dynamic_index_in_dim(doc_pad, position + half_width, 0, keepdims=False)
    next_id = lax.dynamic_index_in_dim(
        doc_pad, position + row_count + half_width + 1, 0, keepdims=False
    )
    summed = jnp.zeros((row_count, conv_all.shape[1]), jnp.float32)
    for offset in range(taps):
        same_doc = (window_ids[offset : offset + row_count] == own_ids)[:, None]
        summed = summed + conv_all[offset] * jnp.where(
            same_doc, extended[offset : offset + row_count], 0.0
        )
    activ = jax.nn.silu(summed)
    values = activ[:, :value_width].reshape(row_count, groups, per_group, HEAD_DIM)
    entries = activ[:, value_width : value_width + state_width].reshape(row_count, groups, STATE)
    readout = activ[:, value_width + state_width :].reshape(row_count, groups, STATE)
    local_parts = []
    for sweep_direction in range(2):
        head_step_length = jax.nn.softplus(
            step_before_softplus.astype(jnp.float32) + head_step_bias[sweep_direction]
        )
        decay_logarithm = (
            -jnp.exp(head_rate_logarithm[sweep_direction]) * head_step_length + sudden_log_decay
        ).reshape(row_count, groups, per_group)
        scaled = values * head_step_length.reshape(row_count, groups, per_group)[..., None]
        arrays = (scaled, entries, readout, decay_logarithm, own_ids)
        edge_id = prev_id
        if sweep_direction == 1:
            arrays = tuple((jnp.flip(array, 0) for array in arrays))
            edge_id = next_id
        start_state = jnp.zeros((groups, per_group, HEAD_DIM, STATE), jnp.float32)
        output, end_state = sweep_blocks(*arrays, start_state, jnp.int32(-1), BLOCK)
        total_decay = jnp.sum(arrays[3], axis=0)
        passing = jnp.where(edge_id == arrays[4][-1], jnp.exp(total_decay), 0.0)
        local_parts.append((arrays, edge_id, output, end_state, passing))
    identity = (
        jnp.ones((groups, per_group), jnp.float32),
        jnp.zeros((groups, per_group, HEAD_DIM, STATE), jnp.float32),
    )
    forward_in = carried_in((local_parts[0][4], local_parts[0][3]), SP, chain, identity, False)[1]
    backward_in = carried_in((local_parts[1][4], local_parts[1][3]), SP, chain, identity, True)[1]
    summed_heads = jnp.zeros((row_count, groups, per_group, HEAD_DIM), jnp.float32)
    for sweep_direction, incoming in ((0, forward_in), (1, backward_in)):
        arrays, edge_id, output, end_state, passing = local_parts[sweep_direction]
        arrival = jnp.where(
            (arrays[4] == edge_id)[:, None, None], jnp.exp(jnp.cumsum(arrays[3], axis=0)), 0.0
        )
        carried = jnp.einsum("tgn,grpn->tgrp", arrays[2], incoming) * arrival[..., None]
        output = output + carried
        if sweep_direction == 1:
            output = jnp.flip(output, 0)
        summed_heads = summed_heads + output
    gated = summed_heads.reshape(row_count, groups, per_group * HEAD_DIM)
    gated = gated * jax.nn.silu(output_gate_rows.astype(jnp.float32)).reshape(
        row_count, groups, per_group * HEAD_DIM
    )
    gated = gated * lax.rsqrt(jnp.mean(gated * gated, axis=2, keepdims=True) + norm_eps)
    normed = (gated.reshape(row_count, value_width) * group_norm_gain).astype(jnp.bfloat16)
    partial_value = jnp.dot(normed, mixer_output_weight, preferred_element_type=jnp.float32)
    mixer_sum = sent_and_summed(partial_value.astype(jnp.bfloat16), "tp", 1)
    first_sum = resid_scale * stream.astype(jnp.float32) + mixer_sum
    normed_one = norm_rows(first_sum, mixer_norm_gain, D)
    up_full, down_full = (
        lax.all_gather(up_projection_weight, SP, axis=0, tiled=True),
        lax.all_gather(down_projection_weight, SP, axis=0, tiled=True),
    )
    hidden = jnp.dot(
        lax.all_gather(normed_one, "tp", axis=1, tiled=True),
        up_full,
        preferred_element_type=jnp.float32,
    )
    squared = jnp.square(jax.nn.relu(hidden)).astype(jnp.bfloat16)
    down_part = lax.dot_general(
        squared, down_full, (((1,), (1,)), ((), ())), preferred_element_type=jnp.float32
    )
    down_sum = lax.psum_scatter(
        down_part.astype(jnp.bfloat16), "tp", scatter_dimension=1, tiled=True
    ).astype(jnp.float32)
    second_sum = resid_scale * normed_one.astype(jnp.float32) + down_sum
    return norm_rows(second_sum, channel_norm_gain, D)


def solution(mesh):
    torus = Mesh(mesh.devices.reshape(8, 4, mesh.shape["tp"]), ("sp_0", "sp_1", "tp"))
    return jax.shard_map(
        per_device,
        mesh=torus,
        in_specs=(
            P(SP, "tp"),
            P(SP, "tp"),
            P(SP, "tp"),
            P(SP, "tp"),
            P(SP, "tp"),
            P(SP, "tp"),
            P(),
            P(None, "tp"),
            P(None, "tp"),
            P(None, "tp"),
            P(None, "tp"),
            P(None, "tp"),
            P("tp"),
            P("tp", None),
            P(SP, "tp"),
            P("tp"),
            P("tp"),
            P(SP, "tp"),
            P(SP, "tp"),
        ),
        out_specs=P(SP, "tp"),
        check_vma=False,
    )
```

profile of v0, /device:TPU:1, one launch (start us, length us, event | category | flops | bytes accessed | tf_op | source)
XLA Modules:
  0.0 508.4 jit_solution(5436518853810099621)
XLA Ops:
  10.4 4.0 collective-permute-start
  24.4 9.6 %all-reduce.5 = (bf16[16]{0:T(256)(128)(2,1)S(1)}, bf16[16]{0:T(256)(128)(2,1)S(1)}) all-reduce(bf16[16]{0:T(256)(128)(2,1)S(1)} %dynamic-update-slice.1, bf16[16]{0:T(256)(128)(2,1)S(1)} %dynamic-update-slice), channel_id=4, replica_groups=mesh['sp_0'=8,'sp_1'=4,'tp'=8] {'sp_1'}, use_global_device_ids=true, to_apply=%add.2 | all-reduce | flops 32 | bytes 128
  36.8 15.4 %all_gather.51 = bf16[8,1,4]{2,1,0:T(2,128)(2,1)S(1)} all-gather(bf16[1,1,4]{2,1,0:T(2,128)(2,1)S(1)} %get-tuple-element.271), channel_id=1, replica_groups=mesh['sp_0'=8,'sp_1'=4,'tp'=8] {'sp_0'}, dimensions={0}, use_global_device_ids=true | all-gather | bytes 72 | tf_op jit(solution)/shard_map/all_gather | solution.py:43
  54.6 10.3 %all_gather.46 = bf16[8,1,4]{2,1,0:T(2,128)(2,1)S(1)} all-gather(bf16[1,1,4]{2,1,0:T(2,128)(2,1)S(1)} %get-tuple-element.269), channel_id=1, replica_groups=mesh['sp_0'=8,'sp_1'=4,'tp'=8] {'sp_0'}, dimensions={0}, use_global_device_ids=true | all-gather | bytes 72 | tf_op jit(solution)/shard_map/all_gather | solution.py:43
  72.2 1.9 divide_multiply_fusion
  76.4 3.6 reverse.11
  80.0 3.6 reverse.12
  84.7 92.6 %while.30 = (s32[]{:T(128)}, f32[1,4,64,128]{3,2,1,0:T(8,128)S(1)}, s32[]{:T(128)}, f32[6,128,1,4,64]{1,0,4,3,2:T(8,128)S(1)}, s32[6,128]{1,0:T(8,128)}, /*index...) while((s32[]{:T(128)}, f32[1,4,64,128]{3,2,1,0:T(8,128)S(1)}, ...), condition=%wide.region_2.3_spmd.clone, body=%wide.region_0.2_spmd.clone.sunk | while | flops 29967624 | bytes 2036490 | solution.py:105
  92.7 1.8 fusion.338
  94.4 3.3 dynamic_update_slice.11
  106.7 1.4 constant_dynamic-slice_fusion.12
  108.1 1.8 fusion.338
  109.9 3.3 dynamic_update_slice.11
  123.5 1.8 fusion.338
  125.3 3.3 dynamic_update_slice.11
  139.0 1.8 fusion.338
  140.8 3.3 dynamic_update_slice.11
  154.4 1.8 fusion.338
  156.2 3.3 dynamic_update_slice.11
  169.9 1.8 fusion.338
  171.6 3.3 dynamic_update_slice.11
  177.4 1.7 broadcast_multiply_fusion.1
  179.1 3.2 rev.19
  183.4 64.5 %while.31 = (s32[]{:T(128)}, f32[1,4,64,128]{3,2,1,0:T(8,128)S(1)}, s32[]{:T(128)}, f32[6,128,1,4,64]{1,0,4,3,2:T(8,128)S(1)}, s32[6,128]{1,0:T(8,128)}, /*index...) while((s32[]{:T(128)}, f32[1,4,64,128]{3,2,1,0:T(8,128)S(1)}, ...), condition=%wide.region_8.9_spmd.clone, body=%wide.region_6.8_spmd.clone.sunk | while | flops 29967624 | bytes 2035982 | solution.py:105
  189.4 2.6 dynamic_update_slice.12
  200.2 2.6 dynamic_update_slice.12
  210.9 2.6 dynamic_update_slice.12
  220.0 1.4 constant_dynamic-slice_fusion.14
  221.7 2.6 dynamic_update_slice.12
  230.8 1.4 constant_dynamic-slice_fusion.14
  232.4 2.6 dynamic_update_slice.12
  243.2 2.6 dynamic_update_slice.12
  247.9 1.4 reshape.1142
  250.5 9.4 %all-gather.3 = bf16[4,4,64,128]{3,2,1,0:T(8,128)(2,1)S(1)} all-gather(bf16[1,4,64,128]{3,2,1,0:T(8,128)(2,1)S(1)} %convert_element_type.693), channel_id=5, replica_groups=mesh['sp_0'=8,'sp_1'=4,'tp'=8] {'sp_1'}, dimensions={0}, use_global_device_ids=true | all-gather | bytes 327680 | tf_op jit(solution)/shard_map/all_gather | solution.py:43
  260.0 19.5 %all_gather.54 = bf16[8,1,4,64,128]{4,3,2,1,0:T(8,128)(2,1)S(1)} all-gather(bf16[1,1,4,64,128]{4,3,2,1,0:T(8,128)(2,1)S(1)} %fusion.137), channel_id=1, replica_groups=mesh['sp_0'=8,'sp_1'=4,'tp'=8] {'sp_0'}, dimensions={0}, use_global_device_ids=true | all-gather | bytes 589824 | tf_op jit(solution)/shard_map/all_gather | solution.py:43
  279.6 2.6 fusion.78
  282.3 3.2 rev.21
  285.4 9.4 %all-gather.1 = bf16[4,4,64,128]{3,2,1,0:T(8,128)(2,1)S(1)} all-gather(bf16[1,4,64,128]{3,2,1,0:T(8,128)(2,1)S(1)} %convert_element_type.649), channel_id=3, replica_groups=mesh['sp_0'=8,'sp_1'=4,'tp'=8] {'sp_1'}, dimensions={0}, use_global_device_ids=true | all-gather | bytes 327680 | tf_op jit(solution)/shard_map/all_gather | solution.py:43
  295.0 19.2 %all_gather.49 = bf16[8,1,4,64,128]{4,3,2,1,0:T(8,128)(2,1)S(1)} all-gather(bf16[1,1,4,64,128]{4,3,2,1,0:T(8,128)(2,1)S(1)} %fusion.170), channel_id=1, replica_groups=mesh['sp_0'=8,'sp_1'=4,'tp'=8] {'sp_0'}, dimensions={0}, use_global_device_ids=true | all-gather | bytes 589824 | tf_op jit(solution)/shard_map/all_gather | solution.py:43
  314.3 2.5 fusion.76
  316.8 1.4 copy.93
  319.9 69.1 %all_to_all.5 = bf16[8,768,256]{2,1,0:T(8,128)(2,1)S(1)} all-to-all(bf16[8,768,256]{2,1,0:T(8,128)(2,1)S(1)} %bitcast.468), channel_id=1, replica_groups=mesh['sp_0'=8,'sp_1'=4,'tp'=8] {'tp'}, dimensions={0} | all-to-all | bytes 6291456 | tf_op jit(solution)/shard_map/all_to_all | solution.py:66
  390.2 13.0 %all-reduce.4 = (f32[768]{0:T(1024)S(1)}, f32[768]{0:T(1024)S(1)}) all-reduce(f32[768]{0:T(1024)S(1)} %get-tuple-element.220, f32[768]{0:T(1024)S(1)} %get-tuple-element.219), channel_id=1, replica_groups=mesh['sp_0'=8,'sp_1'=4,'tp'=8] {'tp'}, use_global_device_ids=true, to_apply=%region_17.18 | all-reduce | flops 1536 | bytes 12288 | tf_op jit(solution)/shard_map/psum | solution.py:114
  404.4 30.3 %all-gather.8.cloned.1.call-done = bf16[768,2048]{1,0:T(8,128)(2,1)} async-done(((bf16[768,256]{1,0:T(8,128)(2,1)}), bf16[768,2048]{1,0:T(8,128)(2,1)}) %all-gather.8.cloned.1.call-update) | async-done | bytes 3145744 | tf_op jit(solution)/shard_map/all_gather | solution.py:225
  434.7 11.9 %convolution_convert_fusion = bf16[768,2048]{1,0:T(8,128)(2,1)} fusion(bf16[2048,1024]{1,0:T(8,128)(2,1)} %all-gather.12.cloned.1.call-done, bf16[768,2048]{1,0:T(8,128)(2,1)} %all-gather.8.cloned.1.call-done, bf16[2048,1024]{1,0:T(8,128)(2,1)} %all-gather.10.cloned.1.call-done), kind=kOutput, calls=%fused_computation.95 | convolution fusion | flops 6446383104 | bytes 14680064 | tf_op jit(solution)/shard_map/dot_general | solution.py:230
  446.7 36.7 %reduce-scatter.2.cloned.1.call-done = bf16[768,256]{1,0:T(8,128)(2,1)} async-done(((bf16[768,2048]{1,0:T(8,128)(2,1)}), bf16[768,256]{1,0:T(8,128)(2,1)}) %reduce-scatter.2.cloned.1.call-update) | async-done | bytes 393232 | tf_op jit(solution)/shard_map/reduce_scatter | solution.py:233
  484.6 15.2 %all-reduce.3 = (f32[768]{0:T(1024)S(1)}, f32[768]{0:T(1024)S(1)}) all-reduce(f32[768]{0:T(1024)S(1)} %get-tuple-element.222, f32[768]{0:T(1024)S(1)} %get-tuple-element.221), channel_id=1, replica_groups=mesh['sp_0'=8,'sp_1'=4,'tp'=8] {'tp'}, use_global_device_ids=true, to_apply=%region_22.23 | all-reduce | flops 1536 | bytes 12288 | tf_op jit(solution)/shard_map/psum | solution.py:114
  499.9 2.0 multiply_convert_fusion.1
  (396 shorter events, 125.2 us)
Async XLA Ops:
  6.5 312.0 %copy-start = (bf16[256,2048]{1,0:T(8,128)(2,1)S(1)}, bf16[256,2048]{1,0:T(8,128)(2,1)}, u32[]{:S(2)}) copy-start(bf16[256,2048]{1,0:T(8,128)(2,1)} %param.36) | copy-start | bytes 3145732
  6.5 16.2 %copy-start.46 = (u32[256]{0:T(256)S(1)}, u32[256]{0:T(256)}, u32[]{:S(2)}) copy-start(u32[256]{0:T(256)} %constant.124) | copy-start | bytes 3076
  6.5 9.3 %copy-start.6 = (s32[24576]{0:T(1024)S(1)}, s32[24576]{0:T(1024)}, u32[]{:S(2)}) copy-start(s32[24576]{0:T(1024)} %param.29) | copy-start | bytes 294916
  6.5 12.0 %copy-start.33 = (f32[2,4]{1,0:T(2,128)S(1)}, f32[2,4]{1,0:T(2,128)}, u32[]{:S(2)}) copy-start(f32[2,4]{1,0:T(2,128)} %param.30) | copy-start | bytes 100
  6.5 12.0 %copy-start.32 = (f32[2,4]{1,0:T(2,128)S(1)}, f32[2,4]{1,0:T(2,128)}, u32[]{:S(2)}) copy-start(f32[2,4]{1,0:T(2,128)} %param.31) | copy-start | bytes 100
  6.5 12.1 %copy-start.12 = (bf16[768,4]{0,1:T(4,128)(2,1)S(1)}, bf16[768,4]{0,1:T(4,128)(2,1)}, u32[]{:S(2)}) copy-start(bf16[768,4]{0,1:T(4,128)(2,1)} %param.27) | copy-start | bytes 18436
  6.6 12.1 %copy-start.11 = (f32[768,4]{0,1:T(4,128)S(1)}, f32[768,4]{0,1:T(4,128)}, u32[]{:S(2)}) copy-start(f32[768,4]{0,1:T(4,128)} %param.28) | copy-start | bytes 36868
  6.6 63.4 %copy-start.17 = (bf16[5,256]{1,0:T(8,128)(2,1)S(1)}, bf16[5,256]{1,0:T(8,128)(2,1)}, u32[]{:S(2)}) copy-start(bf16[5,256]{1,0:T(8,128)(2,1)} %param.32) | copy-start | bytes 7684
  6.6 63.4 %copy-start.31 = (bf16[5,128]{1,0:T(8,128)(2,1)S(1)}, bf16[5,128]{1,0:T(8,128)(2,1)}, u32[]{:S(2)}) copy-start(bf16[5,128]{1,0:T(8,128)(2,1)} %param.33) | copy-start | bytes 3844
  6.6 63.4 %copy-start.30 = (bf16[5,128]{1,0:T(8,128)(2,1)S(1)}, bf16[5,128]{1,0:T(8,128)(2,1)}, u32[]{:S(2)}) copy-start(bf16[5,128]{1,0:T(8,128)(2,1)} %param.34) | copy-start | bytes 3844
  6.6 397.8 %all-gather.10.cloned.1.call-start = ((), (), s32[]{:S(2)}) async-start(), calls=%async_computation.3 | async-start | bytes 4325376 | tf_op jit(solution)/shard_map/all_gather | solution.py:221
  7.3 397.1 %all-gather.12.cloned.1.call-start = ((), (), s32[]{:S(2)}) async-start(), calls=%async_computation.4 | async-start | bytes 4325376 | tf_op jit(solution)/shard_map/all_gather | solution.py:222
  10.4 61.5 %collective-permute-start = (bf16[2,512]{1,0:T(2,128)(2,1)S(1)}, bf16[2,512]{1,0:T(2,128)(2,1)S(1)}, u32[]{:S(2)}, u32[]{:S(2)}) collective-permute-start(bf16[2,512]{1,0:T(2,128)(2,1)S(1)} %get-tuple-element.284), channel_id=1, source_target_pairs={{0,8},{8,16},{16,24},{24,32},{32,40},{40,48},{48,56},{56,64},{64,7... | collective-permute-start | bytes 6152 | tf_op jit(solution)/shard_map/ppermute | solution.py:23
  14.4 57.5 %collective-permute-start.1 = (bf16[2,512]{1,0:T(2,128)(2,1)S(1)}, bf16[2,512]{1,0:T(2,128)(2,1)S(1)}, u32[]{:S(2)}, u32[]{:S(2)}) collective-permute-start(bf16[2,512]{1,0:T(2,128)(2,1)S(1)} %get-tuple-element.285), channel_id=1, source_target_pairs={{8,0},{16,8},{24,16},{32,24},{40,32},{48,40},{56,48},{64,56},{72,6... | collective-permute-start | bytes 6152 | tf_op jit(solution)/shard_map/ppermute | solution.py:26
  15.7 419.0 %all-gather.8.cloned.1.call-start = ((), (), s32[]{:S(2)}) async-start(), calls=%async_computation.2 | async-start | bytes 3538944 | tf_op jit(solution)/shard_map/all_gather | solution.py:225
  177.4 6.0 %copy-start.3 = (f32[6,128,1,4,64]{1,0,4,3,2:T(8,128)}, f32[6,128,1,4,64]{1,0,4,3,2:T(8,128)S(1)}, u32[]{:S(2)}) copy-start(f32[6,128,1,4,64]{1,0,4,3,2:T(8,128)S(1)} %get-tuple-element.101) | copy-start | bytes 2359300
  249.3 10.6 %copy-start.26 = (f32[4]{0:T(128)S(1)}, f32[4]{0:T(128)}, u32[]{:S(2)}) copy-start(f32[4]{0:T(128)} %get-tuple-element.332) | copy-start | bytes 52
  249.3 10.6 %copy-start.27 = (f32[4]{0:T(128)S(1)}, f32[4]{0:T(128)}, u32[]{:S(2)}) copy-start(f32[4]{0:T(128)} %get-tuple-element.333) | copy-start | bytes 52
  249.3 10.6 %copy-start.28 = (f32[4]{0:T(128)S(1)}, f32[4]{0:T(128)}, u32[]{:S(2)}) copy-start(f32[4]{0:T(128)} %get-tuple-element.334) | copy-start | bytes 52
  249.3 10.6 %copy-start.29 = (f32[4]{0:T(128)S(1)}, f32[4]{0:T(128)}, u32[]{:S(2)}) copy-start(f32[4]{0:T(128)} %get-tuple-element.335) | copy-start | bytes 52
  249.4 30.1 %copy-start.10 = (f32[768,4]{0,1:T(4,128)S(1)}, f32[768,4]{0,1:T(4,128)}, u32[]{:S(2)}) copy-start(f32[768,4]{0,1:T(4,128)} %select_bitcast_fusion) | copy-start | bytes 36868
  249.4 30.1 %copy-start.37 = (f32[4]{0:T(128)S(1)}, f32[4]{0:T(128)}, u32[]{:S(2)}) copy-start(f32[4]{0:T(128)} %get-tuple-element.313) | copy-start | bytes 52
  249.4 30.1 %copy-start.38 = (f32[4]{0:T(128)S(1)}, f32[4]{0:T(128)}, u32[]{:S(2)}) copy-start(f32[4]{0:T(128)} %get-tuple-element.314) | copy-start | bytes 52
  249.4 30.1 %copy-start.39 = (f32[4]{0:T(128)S(1)}, f32[4]{0:T(128)}, u32[]{:S(2)}) copy-start(f32[4]{0:T(128)} %get-tuple-element.315) | copy-start | bytes 52
  249.4 30.1 %copy-start.40 = (f32[4]{0:T(128)S(1)}, f32[4]{0:T(128)}, u32[]{:S(2)}) copy-start(f32[4]{0:T(128)} %get-tuple-element.316) | copy-start | bytes 52
  249.4 30.1 %copy-start.41 = (f32[4]{0:T(128)S(1)}, f32[4]{0:T(128)}, u32[]{:S(2)}) copy-start(f32[4]{0:T(128)} %get-tuple-element.317) | copy-start | bytes 52
  249.4 30.1 %copy-start.42 = (f32[4]{0:T(128)S(1)}, f32[4]{0:T(128)}, u32[]{:S(2)}) copy-start(f32[4]{0:T(128)} %get-tuple-element.318) | copy-start | bytes 52
  249.4 30.1 %copy-start.43 = (f32[4]{0:T(128)S(1)}, f32[4]{0:T(128)}, u32[]{:S(2)}) copy-start(f32[4]{0:T(128)} %get-tuple-element.319) | copy-start | bytes 52
  249.5 30.1 %copy-start.44 = (f32[4]{0:T(128)S(1)}, f32[4]{0:T(128)}, u32[]{:S(2)}) copy-start(f32[4]{0:T(128)} %get-tuple-element.331) | copy-start | bytes 52
  249.5 30.1 %copy-start.47 = (f32[4]{0:T(128)S(1)}, f32[4]{0:T(128)}, u32[]{:S(2)}) copy-start(f32[4]{0:T(128)} %fusion.262) | copy-start | bytes 52
  279.6 15.3 %copy-start.13 = (f32[4]{0:T(128)S(1)}, f32[4]{0:T(128)}, u32[]{:S(2)}) copy-start(f32[4]{0:T(128)} %get-tuple-element.327) | copy-start | bytes 52
  279.6 15.3 %copy-start.14 = (f32[4]{0:T(128)S(1)}, f32[4]{0:T(128)}, u32[]{:S(2)}) copy-start(f32[4]{0:T(128)} %get-tuple-element.328) | copy-start | bytes 52
  279.6 15.3 %copy-start.15 = (f32[4]{0:T(128)S(1)}, f32[4]{0:T(128)}, u32[]{:S(2)}) copy-start(f32[4]{0:T(128)} %get-tuple-element.329) | copy-start | bytes 52
  279.6 15.3 %copy-start.16 = (f32[4]{0:T(128)S(1)}, f32[4]{0:T(128)}, u32[]{:S(2)}) copy-start(f32[4]{0:T(128)} %get-tuple-element.330) | copy-start | bytes 52
  282.2 32.0 %copy-start.8 = (f32[768,4]{0,1:T(4,128)S(1)}, f32[768,4]{0,1:T(4,128)}, u32[]{:S(2)}) copy-start(f32[768,4]{0,1:T(4,128)} %select_bitcast_fusion.1) | copy-start | bytes 36868
  282.2 32.0 %copy-start.18 = (f32[4]{0:T(128)S(1)}, f32[4]{0:T(128)}, u32[]{:S(2)}) copy-start(f32[4]{0:T(128)} %get-tuple-element.299) | copy-start | bytes 52
  282.2 32.0 %copy-start.19 = (f32[4]{0:T(128)S(1)}, f32[4]{0:T(128)}, u32[]{:S(2)}) copy-start(f32[4]{0:T(128)} %get-tuple-element.300) | copy-start | bytes 52
  282.2 32.0 %copy-start.20 = (f32[4]{0:T(128)S(1)}, f32[4]{0:T(128)}, u32[]{:S(2)}) copy-start(f32[4]{0:T(128)} %get-tuple-element.301) | copy-start | bytes 52
  282.2 32.0 %copy-start.21 = (f32[4]{0:T(128)S(1)}, f32[4]{0:T(128)}, u32[]{:S(2)}) copy-start(f32[4]{0:T(128)} %get-tuple-element.302) | copy-start | bytes 52
  282.2 32.0 %copy-start.22 = (f32[4]{0:T(128)S(1)}, f32[4]{0:T(128)}, u32[]{:S(2)}) copy-start(f32[4]{0:T(128)} %get-tuple-element.303) | copy-start | bytes 52
  282.2 32.0 %copy-start.23 = (f32[4]{0:T(128)S(1)}, f32[4]{0:T(128)}, u32[]{:S(2)}) copy-start(f32[4]{0:T(128)} %get-tuple-element.304) | copy-start | bytes 52
  282.2 32.0 %copy-start.24 = (f32[4]{0:T(128)S(1)}, f32[4]{0:T(128)}, u32[]{:S(2)}) copy-start(f32[4]{0:T(128)} %get-tuple-element.305) | copy-start | bytes 52
  282.3 32.0 %copy-start.25 = (f32[4]{0:T(128)S(1)}, f32[4]{0:T(128)}, u32[]{:S(2)}) copy-start(f32[4]{0:T(128)} %get-tuple-element.326) | copy-start | bytes 52
  282.3 32.0 %copy-start.36 = (f32[4]{0:T(128)S(1)}, f32[4]{0:T(128)}, u32[]{:S(2)}) copy-start(f32[4]{0:T(128)} %fusion.271) | copy-start | bytes 52
  388.9 14.3 %copy-start.34 = (f32[256]{0:T(256)S(1)}, f32[256]{0:T(256)}, u32[]{:S(2)}) copy-start(f32[256]{0:T(256)} %param.38) | copy-start | bytes 3076
  404.3 79.0 %reduce-scatter.2.cloned.1.call-start = ((), (), s32[]{:S(2)}) async-start(), calls=%async_computation.5 | async-start | bytes 3538944 | tf_op jit(solution)/shard_map/reduce_scatter | solution.py:233
  446.6 36.7 %copy-start.1 = (bf16[768,256]{1,0:T(8,128)(2,1)S(1)}, bf16[768,256]{1,0:T(8,128)(2,1)}, u32[]{:S(2)}) copy-start(bf16[768,256]{1,0:T(8,128)(2,1)} %multiply_convert_fusion.2) | copy-start | bytes 1179652
  446.6 53.3 %copy-start.35 = (f32[256]{0:T(256)S(1)}, f32[256]{0:T(256)}, u32[]{:S(2)}) copy-start(f32[256]{0:T(256)} %param.39) | copy-start | bytes 3076
  (6 other events, 13.8 us)
Sparse Core Ops, SparseCore 0:
  10.0 81.9 all-gather.9
  94.6 78.7 all-gather.11
  404.5 30.2 all-gather.7
  446.8 36.4 reduce-scatter.1
where the time goes:
time: 515 us; the launch traced here: 508 us
  blocking collectives  190 us (37%)
  local copies, waits for them, and re-layouts  111 us (22%)
  waiting for transfers between devices  67.7 us (13%)
  matrix products  58.9 us (11%)
  other arithmetic  41.6 us (8%)
  between operations  17.2 us (3%)
  loops' own time  16.1 us (3%)
  starting transfers between devices  5.47 us (1%)
    all_gather x6, blocking collectives, carried_in(): lax.all_gather(part.astype(kind), axis)  83.1 us
    all_to_all x1, blocking collectives, sent_and_summed(): lax.all_to_all(blocks, axis, split_axis=0, concat_axis=0, tiled=True)  69.1 us
    reduce_scatter x1, waiting for transfers between devices, per_device(): lax.psum_scatter(down_part.astype(jnp.bfloat16), 'tp', scatter_dimension=...  36.7 us
    dynamic_update_slice x12, local copies, waits for them, and re-layouts, sweep_blocks(): lax.scan(block_step, (states, last_doc), inputs)  35.4 us
    all_gather x1, waiting for transfers between devices, per_device(): lax.all_gather(normed_one, 'tp', axis=1, tiled=True)  30.3 us
    psum x2, blocking collectives, norm_rows(): lax.psum((jnp.sum(residual, axis=1), jnp.sum(residual * residual, axis=1)...  28.3 us
    dynamic_slice x24, local copies, waits for them, and re-layouts, sweep_blocks(): lax.scan(block_step, (states, last_doc), inputs)  26.6 us
    another operation x2, loops' own time, sweep_blocks(): lax.scan(block_step, (states, last_doc), inputs)  16.1 us
  transfers between devices with their start and end apart: 6, of which 2 were waited for; matrix products, arithmetic and copies ran while one was open for 38% of the time, Pallas kernels for 0%

commit v1 on v0

v1 whole, which is shorter than its diff:
```python
import functools

import jax
import jax.numpy as jnp
from jax import lax
from jax.experimental import pallas as pl
from jax.experimental.pallas import tpu as pltpu
from jax.sharding import PartitionSpec as P

D = 2048
HEAD_DIM = 64
STATE = 128
REACH = 8
MESH = pl.DeviceIdType.MESH
norm_eps = 1e-05
resid_scale = 1.4142135623730951
F32 = jnp.float32
BF16 = jnp.bfloat16


def lanes_of(cols, rows, base):
    n = rows.size
    low = lax.broadcasted_iota(jnp.int32, (n, 128), 1) < HEAD_DIM
    halves = []
    for k in (0, 2):
        a = jnp.broadcast_to(cols[rows, base + k : base + k + 1], (n, 128))
        b = jnp.broadcast_to(cols[rows, base + k + 1 : base + k + 2], (n, 128))
        halves.append(jnp.where(low, a, b))
    return jnp.concatenate(halves, axis=1)


def head_lanes(column):
    return jnp.concatenate([jnp.broadcast_to(c, (1, HEAD_DIM)) for c in column], axis=1)


C0, D1, W0, W1, A0, A1, DT0, CM, DOC = 0, 4, 8, 12, 16, 20, 24, 28, 33


def mixer_kernel(
    hv, em, rm, gate, per_token, source_mask, taps, gain, out,
    prev_v, prev_e, prev_r, next_v, next_e, next_r,
    wide, rowq, cols, val, ent, ent32, rdo, weight, local,
    msg0, msg1, got0, got1,
    halo_send, halo_recv, state_send, state_recv,
):
    sp, tp = lax.axis_index("sp"), lax.axis_index("tp")
    n_sp = lax.axis_size("sp")
    rows = hv.shape[0]
    tiles = rows // 128

    def at(d):
        return (lax.rem(sp + d + n_sp, n_sp), tp)

    barrier = pltpu.get_barrier_semaphore()
    for d in range(1, REACH + 1):
        for s in (d, -d):
            pl.semaphore_signal(barrier, inc=1, device_id=at(s), device_id_type=MESH)
    pl.semaphore_wait(barrier, 2 * REACH)

    halos = []
    for k, (src, low, high) in enumerate(((hv, prev_v, next_v), (em, prev_e, next_e), (rm, prev_r, next_r))):
        for m, (first, dst, step) in enumerate(((rows - 16, low, 1), (0, high, -1))):
            halos.append(pltpu.make_async_remote_copy(
                src_ref=src.at[pl.ds(first, 16)], dst_ref=dst,
                send_sem=halo_send.at[2 * k + m], recv_sem=halo_recv.at[2 * k + m],
                device_id=at(step), device_id_type=MESH))
    for copy in halos:
        copy.start()

    dt = per_token[0:8, :]
    log_decay = per_token[8:16, :]
    lane = lax.broadcasted_iota(jnp.int32, (8, rows), 1)
    total = log_decay
    shift = 1
    while shift < rows:
        total = total + jnp.where(lane >= shift, pltpu.roll(total, shift, 1), 0.0)
        shift *= 2
    c0 = total[0:4]
    d1 = total[4:8] - log_decay[4:8]
    all0, all1 = total[0:4, rows - 1 : rows], total[4:8, rows - 1 : rows]
    docs = per_token[16:24, :]
    own = docs[2:3]
    same_end = jnp.where(own == own[:, rows - 1 : rows], 1.0, 0.0)
    same_start = jnp.where(own == own[:, 0:1], 1.0, 0.0)
    from_prev = jnp.where(own == docs[5:6], 1.0, 0.0)
    from_next = jnp.where(own == docs[6:7], 1.0, 0.0)
    rowq[...] = jnp.zeros_like(rowq)
    rowq[C0 : C0 + 4, :] = c0
    rowq[D1 : D1 + 4, :] = d1
    rowq[W0 : W0 + 4, :] = jnp.exp(all0 - c0) * dt[0:4] * same_end
    rowq[W1 : W1 + 4, :] = jnp.exp(d1) * dt[4:8] * same_start
    rowq[A0 : A0 + 4, :] = jnp.exp(c0) * from_prev
    rowq[A1 : A1 + 4, :] = jnp.exp(all1 - d1) * from_next
    rowq[DT0 : DT0 + 4, :] = dt[0:4]
    rowq[CM : CM + 5, :] = jnp.where(docs[0:5] == own, 1.0, 0.0)
    rowq[DOC : DOC + 1, :] = own
    for t in range(tiles):
        cols[pl.ds(128 * t, 128), :] = jnp.transpose(rowq[:, 128 * t : 128 * t + 128])

    wide[8 : 8 + rows, 0:256] = hv[...].astype(F32)
    wide[8 : 8 + rows, 256:384] = em[...].astype(F32)
    wide[8 : 8 + rows, 384:512] = rm[...].astype(F32)
    for copy in halos:
        copy.wait()
    wide[0:8, 0:256] = prev_v[8:16, :].astype(F32)
    wide[0:8, 256:384] = prev_e[8:16, :].astype(F32)
    wide[0:8, 384:512] = prev_r[8:16, :].astype(F32)
    wide[8 + rows : 16 + rows, 0:256] = next_v[0:8, :].astype(F32)
    wide[8 + rows : 16 + rows, 256:384] = next_e[0:8, :].astype(F32)
    wide[8 + rows : 16 + rows, 384:512] = next_r[0:8, :].astype(F32)

    for t in range(tiles):
        lo = 128 * t
        masks = [jnp.broadcast_to(cols[lo : lo + 128, CM + o : CM + o + 1], (128, 128)) for o in range(5)]
        for g in range(4):
            acc = jnp.zeros((128, 128), F32)
            for o in range(5):
                part = wide[lo + 6 + o : lo + 134 + o, 128 * g : 128 * g + 128]
                if o != 2:
                    part = part * masks[o]
                acc = acc + taps[o : o + 1, 128 * g : 128 * g + 128] * part
            act = acc * jax.nn.sigmoid(acc)
            if g < 2:
                val[lo : lo + 128, 128 * g : 128 * g + 128] = act.astype(BF16)
            elif g == 2:
                ent32[lo : lo + 128, :] = act
                ent[lo : lo + 128, :] = act.astype(BF16)
            else:
                rdo[lo : lo + 128, :] = act.astype(BF16)

    state0 = jnp.zeros((STATE, 256), F32)
    state1 = jnp.zeros((STATE, 256), F32)
    for t in range(tiles):
        r = pl.ds(128 * t, 128)
        ent_t = jnp.transpose(ent32[r, :]).astype(BF16)
        v = val[r, :].astype(F32)
        state0 += jnp.dot(ent_t, (v * lanes_of(cols, r, W0)).astype(BF16), preferred_element_type=F32)
        state1 += jnp.dot(ent_t, (v * lanes_of(cols, r, W1)).astype(BF16), preferred_element_type=F32)
    for msg, state, whole in ((msg0, state0, all0), (msg1, state1, all1)):
        msg[0:STATE, :] = state.astype(BF16)
        passing = head_lanes([jnp.exp(whole[h : h + 1, :]) for h in range(4)])
        coarse = passing.astype(BF16)
        fine = (passing - coarse.astype(F32)).astype(BF16)
        row = lax.broadcasted_iota(jnp.int32, (16, 256), 0)
        both = jnp.where(row == 0, coarse.astype(F32), jnp.where(row == 1, fine.astype(F32), 0.0))
        msg[STATE : STATE + 16, :] = both.astype(BF16)

    for t in range(tiles):
        r = pl.ds(128 * t, 128)
        own_score = jnp.sum(rdo[r, :].astype(F32) * ent[r, :].astype(F32), axis=1, keepdims=True)
        local[r, :] = own_score * lanes_of(cols, r, DT0) * val[r, :].astype(F32)

    sends = []
    for d in range(1, REACH + 1):
        for m, (msg, got, step) in enumerate(((msg0, got0, d), (msg1, got1, -d))):
            k = 2 * (d - 1) + m
            sends.append(pltpu.make_async_remote_copy(
                src_ref=msg, dst_ref=got.at[d - 1],
                send_sem=state_send.at[k], recv_sem=state_recv.at[k],
                device_id=at(step), device_id_type=MESH))
    for copy in sends:
        copy.start()

    low_lane = lax.broadcasted_iota(jnp.int32, (128, 128), 1) < HEAD_DIM

    def tile_step(i, _):
        r = pl.ds(pl.multiple_of(i * 128, 128), 128)
        here = rdo[r, :]
        doc_t = jnp.broadcast_to(cols[r, DOC : DOC + 1], (128, 128))
        t_index = lax.broadcasted_iota(jnp.int32, (128, 128), 0) + i * 128
        for pair in range(2):
            outs = []
            for h in (2 * pair, 2 * pair + 1):
                ct = jnp.broadcast_to(cols[r, C0 + h : C0 + h + 1], (128, 128))
                dd = jnp.broadcast_to(cols[r, D1 + h : D1 + h + 1], (128, 128))
                for j in range(tiles):
                    s = pl.ds(128 * j, 128)
                    if h == 0:
                        score = lax.dot_general(here, ent[s, :], (((1,), (1,)), ((), ())), preferred_element_type=F32)
                        score = jnp.where(doc_t == per_token[18:19, 128 * j : 128 * j + 128], score, 0.0)
                        weight[1, :, 128 * j : 128 * j + 128] = score
                    score = weight[1, :, 128 * j : 128 * j + 128]
                    s_index = lax.broadcasted_iota(jnp.int32, (128, 128), 1) + 128 * j
                    spread = jnp.minimum(ct - rowq[C0 + h : C0 + h + 1, 128 * j : 128 * j + 128],
                                         rowq[D1 + h : D1 + h + 1, 128 * j : 128 * j + 128] - dd)
                    step = jnp.where(s_index < t_index, per_token[h : h + 1, 128 * j : 128 * j + 128],
                                     per_token[4 + h : 5 + h, 128 * j : 128 * j + 128])
                    weight[0, :, 128 * j : 128 * j + 128] = score * jnp.exp(spread) * step
                outs.append(jnp.dot(weight[0].astype(BF16), val[:, 128 * pair : 128 * pair + 128],
                                    preferred_element_type=F32))
            local[r, 128 * pair : 128 * pair + 128] += jnp.where(low_lane, outs[0], outs[1])
        return 0

    lax.fori_loop(0, tiles, tile_step, 0)

    for copy in sends:
        copy.wait()
    carried = []
    for m, got in enumerate((got0, got1)):
        through = jnp.ones((1, 256), F32)
        state = jnp.zeros((STATE, 256), F32)
        for d in range(1, REACH + 1):
            state = state + got[d - 1, 0:STATE, :].astype(F32) * (through * source_mask[REACH * m + d - 1])
            tail = got[d - 1, STATE : STATE + 16, :].astype(F32)
            through = through * (tail[0:1] + tail[1:2])
        carried.append(state.astype(BF16))

    for t in range(tiles):
        r = pl.ds(128 * t, 128)
        here = rdo[r, :]
        y = local[r, :]
        y += jnp.dot(here, carried[0], preferred_element_type=F32) * lanes_of(cols, r, A0)
        y += jnp.dot(here, carried[1], preferred_element_type=F32) * lanes_of(cols, r, A1)
        z = gate[r, :].astype(F32)
        y = y * (z * jax.nn.sigmoid(z))
        y = y * lax.rsqrt(jnp.mean(y * y, axis=1, keepdims=True) + norm_eps)
        out[r, :] = (y * gain[...]).astype(BF16)


def mixer(hv, em, rm, gate, step, sudden, document_index, rate, bias, tv, te, tr, gain):
    rows = hv.shape[0]
    n_sp = lax.axis_size("sp")
    sp = lax.axis_index("sp")
    raw, sud = step.astype(F32).T, sudden.T
    dts, lds = [], []
    for k in range(2):
        dt = jax.nn.softplus(raw + bias[k][:, None])
        dts.append(dt)
        lds.append(-jnp.exp(rate[k])[:, None] * dt + sud)
    pad = jnp.pad(document_index, 3, constant_values=-1).astype(F32)
    window = lax.dynamic_slice_in_dim(pad, sp * rows, rows + 6)
    shifted = [window[1 + o : 1 + o + rows][None] for o in range(5)]
    before = jnp.broadcast_to(window[2:3], (1, rows))
    after = jnp.broadcast_to(window[rows + 3 : rows + 4], (1, rows))
    per_token = jnp.concatenate(dts + lds + shifted + [before, after, jnp.zeros((1, rows), F32)], axis=0)
    grid = document_index.reshape(n_sp, rows)
    last = lax.dynamic_slice_in_dim(jnp.pad(grid[:, rows - 1], REACH, constant_values=-1), sp, REACH)[::-1]
    first = lax.dynamic_slice_in_dim(jnp.pad(grid[:, 0], REACH, constant_values=-1), sp + REACH + 1, REACH)
    mask = jnp.concatenate([(last == last[0]) & (last >= 0), (first == first[0]) & (first >= 0)]).astype(F32)
    taps = jnp.pad(jnp.concatenate([tv, te, tr], axis=1).astype(F32), ((0, 3), (0, 0)))
    vmem = pl.BlockSpec(memory_space=pltpu.VMEM)
    return pl.pallas_call(
        mixer_kernel,
        out_shape=jax.ShapeDtypeStruct((rows, 256), BF16),
        in_specs=[vmem] * 5 + [pl.BlockSpec(memory_space=pltpu.SMEM)] + [vmem] * 2,
        out_specs=vmem,
        scratch_shapes=[
            pltpu.VMEM((16, 256), BF16), pltpu.VMEM((16, 128), BF16), pltpu.VMEM((16, 128), BF16),
            pltpu.VMEM((16, 256), BF16), pltpu.VMEM((16, 128), BF16), pltpu.VMEM((16, 128), BF16),
            pltpu.VMEM((rows + 16, 512), F32),
            pltpu.VMEM((128, rows), F32),
            pltpu.VMEM((rows, 128), F32),
            pltpu.VMEM((rows, 256), BF16), pltpu.VMEM((rows, 128), BF16), pltpu.VMEM((rows, 128), F32),
            pltpu.VMEM((rows, 128), BF16),
            pltpu.VMEM((2, 128, rows), F32),
            pltpu.VMEM((rows, 256), F32),
            pltpu.VMEM((STATE + 16, 256), BF16), pltpu.VMEM((STATE + 16, 256), BF16),
            pltpu.VMEM((REACH, STATE + 16, 256), BF16), pltpu.VMEM((REACH, STATE + 16, 256), BF16),
            pltpu.SemaphoreType.DMA((6,)), pltpu.SemaphoreType.DMA((6,)),
            pltpu.SemaphoreType.DMA((2 * REACH,)), pltpu.SemaphoreType.DMA((2 * REACH,)),
        ],
        compiler_params=pltpu.CompilerParams(
            collective_id=0, has_side_effects=True, vmem_limit_bytes=40 * 1024 * 1024),
        cost_estimate=pl.CostEstimate(flops=2_000_000_000, bytes_accessed=3_000_000, transcendentals=0),
        name="mixer",
    )(hv, em, rm, gate, per_token, mask, taps, gain[None, :])


def cut_along(array, dim, count):
    dims = array.shape
    blocks = array.reshape(*dims[:dim], count, dims[dim] // count, *dims[dim + 1 :])
    return jnp.moveaxis(blocks, dim, 0)


def sent_and_summed(array, axis, dim):
    blocks = cut_along(array, dim, lax.axis_size(axis))
    arrived = lax.all_to_all(blocks, axis, split_axis=0, concat_axis=0, tiled=True)
    return arrived.astype(jnp.float32).sum(axis=0)


def norm_rows(residual, gain, width):
    sums = lax.psum((jnp.sum(residual, axis=1), jnp.sum(residual * residual, axis=1)), "tp")
    row_mean = sums[0] / width
    row_var = sums[1] / width - row_mean * row_mean
    return ((residual - row_mean[:, None]) * lax.rsqrt(row_var + norm_eps)[:, None] * gain).astype(
        jnp.bfloat16
    )


def per_device(hv, em, rm, gate, step, sudden, document_index, rate, bias, tv, te, tr, gain,
               mixer_output_weight, stream, mixer_norm_gain, channel_norm_gain, up, down):
    normed = mixer(hv, em, rm, gate, step, sudden, document_index, rate, bias, tv, te, tr, gain)
    partial_value = jnp.dot(normed, mixer_output_weight, preferred_element_type=jnp.float32)
    mixer_sum = sent_and_summed(partial_value.astype(jnp.bfloat16), "tp", 1)
    first_sum = resid_scale * stream.astype(jnp.float32) + mixer_sum
    normed_one = norm_rows(first_sum, mixer_norm_gain, D)
    up_full, down_full = (
        lax.all_gather(up, "sp", axis=0, tiled=True),
        lax.all_gather(down, "sp", axis=0, tiled=True),
    )
    hidden = jnp.dot(
        lax.all_gather(normed_one, "tp", axis=1, tiled=True),
        up_full,
        preferred_element_type=jnp.float32,
    )
    squared = jnp.square(jax.nn.relu(hidden)).astype(jnp.bfloat16)
    down_part = lax.dot_general(
        squared, down_full, (((1,), (1,)), ((), ())), preferred_element_type=jnp.float32
    )
    down_sum = lax.psum_scatter(
        down_part.astype(jnp.bfloat16), "tp", scatter_dimension=1, tiled=True
    ).astype(jnp.float32)
    second_sum = resid_scale * normed_one.astype(jnp.float32) + down_sum
    return norm_rows(second_sum, channel_norm_gain, D)


SPECS = (
    P("sp", "tp"), P("sp", "tp"), P("sp", "tp"), P("sp", "tp"), P("sp", "tp"), P("sp", "tp"), P(),
    P(None, "tp"), P(None, "tp"), P(None, "tp"), P(None, "tp"), P(None, "tp"), P("tp"),
    P("tp", None), P("sp", "tp"), P("tp"), P("tp"), P("sp", "tp"), P("sp", "tp"),
)


def solution(mesh):
    return jax.shard_map(per_device, mesh=mesh, in_specs=SPECS, out_specs=P("sp", "tp"), check_vma=False)
```

time: 515 us -> 287 us (0.56); the launches traced: 508 us -> 286 us
  blocking collectives: 190 us -> 72.5 us
  local copies, waits for them, and re-layouts: 111 us -> 9.33 us
  waiting for transfers between devices: 67.7 us -> 129 us
  matrix products: 58.9 us -> 12.9 us
  Pallas kernels: 0 us -> 40.4 us
  other arithmetic: 41.6 us -> 8.95 us
  loops' own time: 16.1 us -> 0 us
  starting transfers between devices: 5.47 us -> 0.3 us
    all_gather x6 -> x0, blocking collectives: 83.1 us -> none  [carried_in(): lax.all_gather(part.astype(kind), axis)]
    all_gather x2, waiting for transfers between devices: 0.04 us -> 54.5 us  [the longest x1 54.4 us: per_device(): lax.all_gather(down, 'sp', axis=0, tiled=True)]
    dot_general x50 -> x0, matrix products: 45.9 us -> none  [the longest x12 12.3 us: block_step(): within = jnp.einsum('tsg,tsgr,sgrp->tgrp', scores, weights, scaled)]
    pallas_call x0 -> x1, Pallas kernels: none -> 40.4 us  [mixer(): pl.pallas_call(mixer_kernel, out_shape=jax.ShapeDtypeStruct((rows, 256),...]
    dynamic_update_slice x12 -> x0, local copies, waits for them, and re-layouts: 35.4 us -> none  [sweep_blocks(): lax.scan(block_step, (states, last_doc), inputs)]
    dynamic_slice x26 -> x1, local copies, waits for them, and re-layouts: 27.3 us -> 0.09 us  [mixer(): lax.dynamic_slice_in_dim(jnp.pad(grid[:, 0], REACH, constant_values=-1),...]
    all_to_all x1, blocking collectives: 69.1 us -> 43.8 us  [sent_and_summed(): lax.all_to_all(blocks, axis, split_axis=0, concat_axis=0, tiled=True)]
    another operation x40 -> x0, local copies, waits for them, and re-layouts: 18.7 us -> none
  transfers between devices with their start and end apart: 6 -> 4, of which waited for: 2 -> 3; matrix products, arithmetic and copies ran while one was open for 38% -> 4% of each run, Pallas kernels for 0% -> 14%
where the time goes in v1:
time: 287 us; the launch traced here: 286 us
  waiting for transfers between devices  129 us (45%)
  blocking collectives  72.5 us (25%)
  Pallas kernels  40.4 us (14%)
  between operations  13.3 us (5%)
  matrix products  12.9 us (4%)
  local copies, waits for them, and re-layouts  9.33 us (3%)
  other arithmetic  8.95 us (3%)
    all_gather x1, waiting for transfers between devices, per_device(): lax.all_gather(down, 'sp', axis=0, tiled=True)  54.4 us
    all_to_all x1, blocking collectives, sent_and_summed(): lax.all_to_all(blocks, axis, split_axis=0, concat_axis=0, tiled=True)  43.8 us
    pallas_call x1, Pallas kernels, mixer(): pl.pallas_call(mixer_kernel, out_shape=jax.ShapeDtypeStruct((rows, 256),...  40.4 us
    reduce_scatter x1, waiting for transfers between devices, per_device(): lax.psum_scatter(down_part.astype(jnp.bfloat16), 'tp', scatter_dimension=...  36.7 us
    all_gather x1, waiting for transfers between devices, per_device(): lax.all_gather(normed_one, 'tp', axis=1, tiled=True)  36.2 us
    psum x2, blocking collectives, norm_rows(): lax.psum((jnp.sum(residual, axis=1), jnp.sum(residual * residual, axis=1)...  28.7 us
    dot_general x1, matrix products, per_device(): lax.dot_general(squared, down_full, (((1,), (1,)), ((), ())), preferred_e...  11.9 us
  transfers between devices with their start and end apart: 4, of which 3 were waited for; matrix products, arithmetic and copies ran while one was open for 4% of the time, Pallas kernels for 14%

profile of v1, /device:TPU:1, one launch (start us, length us, event | category | flops | bytes accessed | tf_op | source)
XLA Modules:
  0.0 286.5 jit_solution(17566429057320686004)
XLA Ops:
  6.5 0.0 all-gather.6.cloned.1.call-start
  6.5 0.7 all-gather.6.cloned.1.call-update
  7.3 0.0 all-gather.8.cloned.1.call-start
  7.3 0.7 all-gather.8.cloned.1.call-update
  8.0 0.0 all-gather.4.cloned.1.call-start
  8.1 0.9 reshape.38
  9.0 0.2 slice_reduce_fusion.1
  9.2 0.1 pad_dynamic-slice_fusion.1
  9.2 0.7 slice.64
  9.9 0.1 rev.3
  10.0 0.8 fusion.22
  10.8 0.1 fusion.25
  10.9 0.6 fusion.24
  11.5 0.8 negate_bitcast_fusion
  12.3 0.8 bitcast_add_fusion
  13.1 0.7 broadcast_in_dim.45
  13.8 0.6 broadcast_in_dim.44
  14.4 0.1 concatenate.9.per_token
  14.6 0.7 compare_and_fusion.1
  15.3 0.1 add_convert_fusion.source_mask
  15.3 0.7 fusion.21.taps
  16.1 1.0 copy-done.1
  17.1 1.0 copy-done.2
  18.1 0.9 copy-done.3
  19.0 0.9 copy-done.4
  19.9 0.7 copy-done.5
  20.6 40.4 %mixer.1 = bf16[768,256]{1,0:T(8,128)(2,1)S(1)} custom-call(bf16[768,256]{1,0:T(8,128)(2,1)S(1)} %copy-done.1, bf16[768,128]{1,0:T(8,128)(2,1)S(1)} %copy-done.3, bf16[768,128]{1,0:T(8,128)(2,1)S(1)} %copy-done.4, bf16[768,256]{1,0:T(8,128)(2,1)S(1)} %copy-done.2, f32[24,768]{1,0:T(8,128)S(1)} %concatenate.9.per_token, f32[16]{0:T(128)S(1)} %add_convert_fusion.source_mask, ...), custom_call_target="tpu_custom_call" | custom-call | flops 2000000000 | bytes 3000000 | tf_op jit(solution)/shard_map/mixer/pallas_call | solution.py:242
  61.0 0.0 copy-done
  61.0 1.0 convolution_convert_fusion.1
  62.0 0.2 copy.23
  62.2 43.8 %all_to_all.5 = bf16[8,768,256]{2,1,0:T(8,128)(2,1)S(1)} all-to-all(bf16[8,768,256]{2,1,0:T(8,128)(2,1)S(1)} %bitcast.73), channel_id=1, replica_groups=mesh['sp'=32,'tp'=8] {'tp'}, dimensions={0} | all-to-all | bytes 6291456 | tf_op jit(solution)/shard_map/all_to_all | solution.py:277
  106.1 0.4 convert_reduce_fusion
  106.5 0.5 copy-done.7
  107.0 0.3 fusion.1
  107.3 13.4 %all-reduce.5 = (f32[768]{0:T(1024)S(1)}, f32[768]{0:T(1024)S(1)}) all-reduce(f32[768]{0:T(1024)S(1)} %get-tuple-element.6, f32[768]{0:T(1024)S(1)} %get-tuple-element.5), channel_id=1, replica_groups=mesh['sp'=32,'tp'=8] {'tp'}, use_global_device_ids=true, to_apply=%region_4.5 | all-reduce | flops 1536 | bytes 12288 | tf_op jit(solution)/shard_map/psum | solution.py:282
  120.8 1.0 multiply_convert_fusion.2
  121.8 0.0 all-gather.4.cloned.1.call-update
  121.8 0.2 reduce-scatter.2.cloned.1.call-start
  122.1 0.0 all-gather.6.cloned.1.call-done
  122.1 54.4 %all-gather.8.cloned.1.call-done = bf16[2048,1024]{1,0:T(8,128)(2,1)} async-done(((bf16[64,1024]{1,0:T(8,128)(2,1)}), bf16[2048,1024]{1,0:T(8,128)(2,1)}) %all-gather.8.cloned.1.call-update) | async-done | bytes 4194320 | tf_op jit(solution)/shard_map/all_gather | solution.py:299
  176.5 36.2 %all-gather.4.cloned.1.call-done = bf16[768,2048]{1,0:T(8,128)(2,1)} async-done(((bf16[768,256]{1,0:T(8,128)(2,1)}), bf16[768,2048]{1,0:T(8,128)(2,1)}) %all-gather.4.cloned.1.call-update) | async-done | bytes 3145744 | tf_op jit(solution)/shard_map/all_gather | solution.py:302
  212.8 11.9 %convolution_convert_fusion = bf16[768,2048]{1,0:T(8,128)(2,1)} fusion(bf16[2048,1024]{1,0:T(8,128)(2,1)} %all-gather.8.cloned.1.call-done, bf16[768,2048]{1,0:T(8,128)(2,1)} %all-gather.4.cloned.1.call-done, bf16[2048,1024]{1,0:T(8,128)(2,1)} %all-gather.6.cloned.1.call-done), kind=kOutput, calls=%fused_computation.1 | convolution fusion | flops 6446383104 | bytes 14680064 | tf_op jit(solution)/shard_map/dot_general | solution.py:307
  224.6 0.0 reduce-scatter.2.cloned.1.call-update
  224.7 36.7 %reduce-scatter.2.cloned.1.call-done = bf16[768,256]{1,0:T(8,128)(2,1)} async-done(((bf16[768,2048]{1,0:T(8,128)(2,1)}), bf16[768,256]{1,0:T(8,128)(2,1)}) %reduce-scatter.2.cloned.1.call-update) | async-done | bytes 393232 | tf_op jit(solution)/shard_map/reduce_scatter | solution.py:310
  261.3 0.0 copy-done.6
  261.3 1.3 fusion
  262.6 15.2 %all-reduce.4 = (f32[768]{0:T(1024)S(1)}, f32[768]{0:T(1024)S(1)}) all-reduce(f32[768]{0:T(1024)S(1)} %get-tuple-element.8, f32[768]{0:T(1024)S(1)} %get-tuple-element.7), channel_id=1, replica_groups=mesh['sp'=32,'tp'=8] {'tp'}, use_global_device_ids=true, to_apply=%region_9.10 | all-reduce | flops 1536 | bytes 12288 | tf_op jit(solution)/shard_map/psum | solution.py:282
  277.9 2.0 multiply_convert_fusion.1
  (21 shorter events, 0.1 us)
Async XLA Ops:
  6.5 54.5 %copy-start = (bf16[256,2048]{1,0:T(8,128)(2,1)S(1)}, bf16[256,2048]{1,0:T(8,128)(2,1)}, u32[]{:S(2)}) copy-start(bf16[256,2048]{1,0:T(8,128)(2,1)} %param.32) | copy-start | bytes 3145732
  6.5 115.5 %all-gather.6.cloned.1.call-start = ((), (), s32[]{:S(2)}) async-start(), calls=%async_computation.3 | async-start | bytes 4325376 | tf_op jit(solution)/shard_map/all_gather | solution.py:298
  7.3 169.3 %all-gather.8.cloned.1.call-start = ((), (), s32[]{:S(2)}) async-start(), calls=%async_computation.4 | async-start | bytes 4325376 | tf_op jit(solution)/shard_map/all_gather | solution.py:299
  8.0 204.7 %all-gather.4.cloned.1.call-start = ((), (), s32[]{:S(2)}) async-start(), calls=%async_computation.2 | async-start | bytes 3538944 | tf_op jit(solution)/shard_map/all_gather | solution.py:302
  16.1 1.0 copy-start.1
  17.1 1.0 copy-start.2
  18.1 0.9 copy-start.3
  19.0 0.9 copy-start.4
  19.9 0.7 copy-start.5
  106.0 1.0 copy-start.7
  106.1 14.7 %copy-start.8 = (f32[256]{0:T(256)S(1)}, f32[256]{0:T(256)}, u32[]{:S(2)}) copy-start(f32[256]{0:T(256)} %param.34) | copy-start | bytes 3076
  121.8 139.5 %reduce-scatter.2.cloned.1.call-start = ((), (), s32[]{:S(2)}) async-start(), calls=%async_computation.5 | async-start | bytes 3538944 | tf_op jit(solution)/shard_map/reduce_scatter | solution.py:310
  224.6 36.7 %copy-start.6 = (bf16[768,256]{1,0:T(8,128)(2,1)S(1)}, bf16[768,256]{1,0:T(8,128)(2,1)}, u32[]{:S(2)}) copy-start(bf16[768,256]{1,0:T(8,128)(2,1)} %multiply_convert_fusion.2) | copy-start | bytes 1179652
  224.6 53.3 %copy-start.9 = (f32[256]{0:T(256)S(1)}, f32[256]{0:T(256)}, u32[]{:S(2)}) copy-start(f32[256]{0:T(256)} %param.35) | copy-start | bytes 3076
Sparse Core Ops, SparseCore 0:
  9.9 85.3 all-gather.5
  97.9 78.5 all-gather.7
  178.4 34.3 all-gather.3
  224.8 36.4 reduce-scatter.1

commit v2 on v1

--- a/solution.py
+++ b/solution.py
@@ -36,36 +36,239 @@
 C0, D1, W0, W1, A0, A1, DT0, CM, DOC = 0, 4, 8, 12, 16, 20, 24, 28, 33
 
 
-def mixer_kernel(
-    hv, em, rm, gate, per_token, source_mask, taps, gain, out,
+def copy_to(src, dst, send, recv, device):
+    return pltpu.make_async_remote_copy(src_ref=src, dst_ref=dst, send_sem=send, recv_sem=recv,
+                                        device_id=device, device_id_type=MESH)
+
+
+class WeightRing:
+    def __init__(self, up_in, down_in, up, down, sems, sp, tp):
+        (self.uy_s, self.uy_r, self.uh_s, self.uh_r, self.uz_s, self.uz_r,
+         self.dz_s, self.dz_r, self.dy_s, self.dy_r, self.dh_s, self.dh_r) = sems
+        self.up_in, self.down_in, self.up, self.down, self.tp = up_in, down_in, up, down, tp
+        self.y, self.z = lax.rem(sp, 4), sp // 4
+        self.sent = []
+
+    def dev(self, dz, dy):
+        return (lax.rem(self.z + dz + 8, 8) * 4 + lax.rem(self.y + dy + 4, 4), self.tp)
+
+    def rows(self, dz, dy, low=0, count=64):
+        shard = lax.rem(self.z + dz + 8, 8) * 4 + lax.rem(self.y + dy + 4, 4)
+        return pl.ds(pl.multiple_of(shard * 64 + low, 32), count)
+
+    def send(self, src, dst, send, recv, device):
+        copy = copy_to(src, dst, send, recv, device)
+        copy.start()
+        self.sent.append(copy)
+
+    def arrived(self, dst, send, recv):
+        copy_to(dst, dst, send, recv, self.dev(1, 0)).wait_recv()
+
+    def up_z(self, s, p, receive):
+        for m, sign in enumerate((1, -1)):
+            low, count = (32 * m, 32) if s == 3 else (0, 64)
+            if receive:
+                r = self.rows(-sign * (s + 1), p, low, count)
+                self.arrived(self.up.at[r], self.uz_s.at[m, s, p], self.uz_r.at[m, s, p])
+            else:
+                r = self.rows(-sign * s, p, low, count)
+                src = self.up_in if s == 0 and p == 0 else self.up.at[r]
+                self.send(src, self.up.at[r], self.uz_s.at[m, s, p], self.uz_r.at[m, s, p], self.dev(sign, 0))
+
+    def down_z(self, s, receive):
+        for m, sign in enumerate((1, -1)):
+            low, count = (32 * m, 32) if s == 3 else (0, 64)
+            if receive:
+                r = self.rows(-sign * (s + 1), 0, low, count)
+                self.arrived(self.down.at[r], self.dz_s.at[m, s], self.dz_r.at[m, s])
+            else:
+                r = self.rows(-sign * s, 0, low, count)
+                src = self.down_in if s == 0 else self.down.at[r]
+                self.send(src, self.down.at[r], self.dz_s.at[m, s], self.dz_r.at[m, s], self.dev(sign, 0))
+
+    def planes(self, s):
+        return [(0, 0)] if s == 0 else [(7, 4)] if s == 4 else [(2 * s - 1, -s), (2 * s, s)]
+
+    def down_y(self, s):
+        for k, dz in self.planes(s):
+            for m, sign in enumerate((1, -1)):
+                r = self.rows(dz, 0)
+                src = self.down_in if s == 0 else self.down.at[r]
+                self.send(src, self.down.at[r], self.dy_s.at[k, m], self.dy_r.at[k, m], self.dev(0, sign))
+
+    def down_half(self, s, receive):
+        for k, dz in self.planes(s):
+            for m, sign in enumerate((1, -1)):
+                if receive:
+                    r = self.rows(dz, -2 * sign, 32 * m, 32)
+                    self.arrived(self.down.at[r], self.dh_s.at[k, m], self.dh_r.at[k, m])
+                else:
+                    self.arrived(self.down.at[self.rows(dz, -sign)], self.dy_s.at[k, m], self.dy_r.at[k, m])
+                    r = self.rows(dz, -sign, 32 * m, 32)
+                    self.send(self.down.at[r], self.down.at[r], self.dh_s.at[k, m], self.dh_r.at[k, m],
+                              self.dev(0, sign))
+
+    def step(self, n):
+        s, part = divmod(n, 3)
+        if part == 0:
+            if s == 0:
+                for m, sign in enumerate((1, -1)):
+                    self.send(self.up_in, self.up.at[self.rows(0, 0)], self.uy_s.at[m], self.uy_r.at[m],
+                              self.dev(0, sign))
+            else:
+                self.up_z(s - 1, 0, True)
+                self.down_z(s - 1, True)
+            if s < 4:
+                self.up_z(s, 0, False)
+                self.down_z(s, False)
+            self.down_y(s)
+        elif part == 1:
+            if s == 0:
+                for m, sign in enumerate((1, -1)):
+                    self.arrived(self.up.at[self.rows(0, -sign)], self.uy_s.at[m], self.uy_r.at[m])
+                    r = self.rows(0, -sign, 32 * m, 32)
+                    self.send(self.up.at[r], self.up.at[r], self.uh_s.at[m], self.uh_r.at[m], self.dev(0, sign))
+            else:
+                self.up_z(s - 1, 1, True)
+                self.up_z(s - 1, 3, True)
+            if s < 4:
+                self.up_z(s, 1, False)
+                self.up_z(s, 3, False)
+            self.down_half(s, False)
+        else:
+            if s == 0:
+                for m, sign in enumerate((1, -1)):
+                    self.arrived(self.up.at[self.rows(0, -2 * sign, 32 * m, 32)], self.uh_s.at[m], self.uh_r.at[m])
+            else:
+                self.up_z(s - 1, 2, True)
+            if s < 4:
+                self.up_z(s, 2, False)
+
+    def finish(self):
+        for s in range(5):
+            self.down_half(s, True)
+
+
+class TpGather:
+    def __init__(self, own, buf, size, send, recv, sp, tp):
+        self.own, self.buf, self.size, self.s, self.r, self.sp = own, buf, size, send, recv, sp
+        self.x, self.c = tp // 2, lax.rem(tp, 2)
+        self.sent = []
+
+    def slot(self, dx, other):
+        return lax.rem(self.x + dx + 4, 4) * 2 + (1 - self.c if other else self.c)
+
+    def rows(self, dx, other, half=None):
+        low, count = (0, self.size) if half is None else (half * (self.size // 2), self.size // 2)
+        return self.buf.at[pl.ds(pl.multiple_of(self.slot(dx, other) * self.size + low, 16), count)]
+
+    def send(self, src, dst, k, dx, other):
+        copy = copy_to(src, dst, self.s.at[k], self.r.at[k], (self.sp, self.slot(dx, other)))
+        copy.start()
+        self.sent.append(copy)
+
+    def arrived(self, dst, k):
+        copy_to(dst, dst, self.s.at[k], self.r.at[k], (self.sp, self.slot(0, True))).wait_recv()
+
+    def begin(self):
+        mine = self.rows(0, False)
+        self.send(self.own, mine, 0, 1, False)
+        self.send(self.own, mine, 1, -1, False)
+        self.send(self.own, mine, 2, 0, True)
+
+    def relay(self):
+        left, right = self.rows(-1, False), self.rows(1, False)
+        self.arrived(left, 0)
+        self.send(self.rows(-1, False, 0), self.rows(-1, False, 0), 3, 1, False)
+        self.send(left, left, 5, 0, True)
+        self.arrived(right, 1)
+        self.send(self.rows(1, False, 1), self.rows(1, False, 1), 4, -1, False)
+        self.send(right, right, 6, 0, True)
+
+    def far(self):
+        self.arrived(self.rows(2, False, 0), 3)
+        self.arrived(self.rows(2, False, 1), 4)
+        self.send(self.rows(2, False), self.rows(2, False), 7, 0, True)
+
+    def sibling(self, k):
+        self.arrived(self.rows({2: 0, 5: -1, 6: 1, 7: 2}[k], True), k)
+
+
+def layer_kernel(
+    hv, em, rm, gate, per_token, source_mask, taps, gain, up_in, down_in, wout_in, stream, gains_in, last_gain, out,
     prev_v, prev_e, prev_r, next_v, next_e, next_r,
     wide, rowq, cols, val, ent, ent32, rdo, weight, local,
     msg0, msg1, got0, got1,
+    up, down, wout, norm_out, norm_in, stream_in, gains, first, tok, squares,
+    sib_out, sib_in, own_part, outgoing, parts, stat_out, stat_in,
     halo_send, halo_recv, state_send, state_recv,
+    uy_s, uy_r, uh_s, uh_r, uz_s, uz_r, dz_s, dz_r, dy_s, dy_r, dh_s, dh_r,
+    wo_s, wo_r, tk_s, tk_r, ex_s, ex_r, sb_s, sb_r, rs_s, rs_r, st_s, st_r,
 ):
     sp, tp = lax.axis_index("sp"), lax.axis_index("tp")
     n_sp = lax.axis_size("sp")
+    n_tp = lax.axis_size("tp")
     rows = hv.shape[0]
     tiles = rows // 128
+    share = rows // n_tp
 
     def at(d):
         return (lax.rem(sp + d + n_sp, n_sp), tp)
+
+    def peer(d):
+        return lax.rem(tp + d + n_tp, n_tp)
 
     barrier = pltpu.get_barrier_semaphore()
     for d in range(1, REACH + 1):
         for s in (d, -d):
             pl.semaphore_signal(barrier, inc=1, device_id=at(s), device_id_type=MESH)
-    pl.semaphore_wait(barrier, 2 * REACH)
+    for d in range(1, n_tp):
+        pl.semaphore_signal(barrier, inc=1, device_id=(sp, peer(d)), device_id_type=MESH)
+    pl.semaphore_wait(barrier, 2 * REACH + n_tp - 1)
 
     halos = []
     for k, (src, low, high) in enumerate(((hv, prev_v, next_v), (em, prev_e, next_e), (rm, prev_r, next_r))):
-        for m, (first, dst, step) in enumerate(((rows - 16, low, 1), (0, high, -1))):
-            halos.append(pltpu.make_async_remote_copy(
-                src_ref=src.at[pl.ds(first, 16)], dst_ref=dst,
-                send_sem=halo_send.at[2 * k + m], recv_sem=halo_recv.at[2 * k + m],
-                device_id=at(step), device_id_type=MESH))
+        for m, (start, dst, step) in enumerate(((rows - 16, low, 1), (0, high, -1))):
+            halos.append(copy_to(src.at[pl.ds(start, 16)], dst, halo_send.at[2 * k + m], halo_recv.at[2 * k + m],
+                                 at(step)))
     for copy in halos:
         copy.start()
+    ring = WeightRing(up_in, down_in, up, down,
+                      (uy_s, uy_r, uh_s, uh_r, uz_s, uz_r, dz_s, dz_r, dy_s, dy_r, dh_s, dh_r), sp, tp)
+    ring.step(0)
+    wo = TpGather(wout_in, wout, 256, wo_s, wo_r, sp, tp)
+    wo.begin()
+
+    def my_lanes(ref, q):
+        return ref.at[:, pl.ds(pl.multiple_of(q * 256, 256), 256)]
+
+    def exchange(k, src_of, dst):
+        sent = []
+        for d in range(1, n_tp):
+            q = peer(d)
+            copy = copy_to(src_of(q), my_lanes(dst, tp), ex_s.at[k, d - 1], ex_r.at[k, d - 1], (sp, q))
+            copy.start()
+            sent.append(copy)
+        return sent
+
+    def exchanged(k, dst):
+        for d in range(1, n_tp):
+            r = my_lanes(dst, peer(-d))
+            copy_to(r, r, ex_s.at[k, d - 1], ex_r.at[k, d - 1], (sp, peer(d))).wait_recv()
+
+    def token_rows(ref):
+        return lambda q: ref.at[pl.ds(pl.multiple_of(q * share, 16), share)]
+
+    sends = exchange(0, token_rows(stream), stream_in)
+    sends += exchange(1, lambda q: gains_in, gains)
+    mine = pl.ds(pl.multiple_of(tp * share, 16), share)
+    my_cols = pl.ds(pl.multiple_of(tp * 256, 256), 256)
+    own_rows = pl.ds(pl.multiple_of(sp * 64, 64), 64)
+    stream_in[:, my_cols] = stream[mine, :]
+    gains[:, my_cols] = gains_in[...]
+    up[own_rows, :] = up_in[...]
+    down[own_rows, :] = down_in[...]
+    wout[pl.ds(pl.multiple_of(tp * 256, 256), 256), :] = wout_in[...]
 
     dt = per_token[0:8, :]
     log_decay = per_token[8:16, :]
@@ -128,6 +331,8 @@
             else:
                 rdo[lo : lo + 128, :] = act.astype(BF16)
 
+    ring.step(1)
+    ring.step(2)
     state0 = jnp.zeros((STATE, 256), F32)
     state1 = jnp.zeros((STATE, 256), F32)
     for t in range(tiles):
@@ -150,16 +355,17 @@
         own_score = jnp.sum(rdo[r, :].astype(F32) * ent[r, :].astype(F32), axis=1, keepdims=True)
         local[r, :] = own_score * lanes_of(cols, r, DT0) * val[r, :].astype(F32)
 
-    sends = []
+    state_sends = []
     for d in range(1, REACH + 1):
         for m, (msg, got, step) in enumerate(((msg0, got0, d), (msg1, got1, -d))):
             k = 2 * (d - 1) + m
-            sends.append(pltpu.make_async_remote_copy(
+            state_sends.append(pltpu.make_async_remote_copy(
                 src_ref=msg, dst_ref=got.at[d - 1],
                 send_sem=state_send.at[k], recv_sem=state_recv.at[k],
                 device_id=at(step), device_id_type=MESH))
-    for copy in sends:
+    for copy in state_sends:
         copy.start()
+    ring.step(3)
 
     low_lane = lax.broadcasted_iota(jnp.int32, (128, 128), 1) < HEAD_DIM
 
@@ -191,9 +397,13 @@
             local[r, 128 * pair : 128 * pair + 128] += jnp.where(low_lane, outs[0], outs[1])
         return 0
 
-    lax.fori_loop(0, tiles, tile_step, 0)
-
-    for copy in sends:
+    lax.fori_loop(0, tiles // 2, tile_step, 0)
+    ring.step(4)
+    lax.fori_loop(tiles // 2, tiles, tile_step, 0)
+    ring.step(5)
+    ring.step(6)
+
+    for copy in state_sends:
         copy.wait()
     carried = []
     for m, got in enumerate((got0, got1)):
@@ -214,10 +424,127 @@
         z = gate[r, :].astype(F32)
         y = y * (z * jax.nn.sigmoid(z))
         y = y * lax.rsqrt(jnp.mean(y * y, axis=1, keepdims=True) + norm_eps)
-        out[r, :] = (y * gain[...]).astype(BF16)
-
-
-def mixer(hv, em, rm, gate, step, sudden, document_index, rate, bias, tv, te, tr, gain):
+        norm_out[r, :] = (y * gain[...]).astype(BF16)
+
+    norm_in[:, my_cols] = norm_out[mine, :]
+    sends += exchange(2, token_rows(norm_out), norm_in)
+    ring.step(7)
+    ring.step(8)
+    wo.relay()
+    exchanged(0, stream_in)
+    exchanged(1, gains)
+    exchanged(2, norm_in)
+    ring.step(9)
+    wo.far()
+    for k in (2, 5, 6, 7):
+        wo.sibling(k)
+    for n in range(4):
+        c = pl.ds(512 * n, 512)
+        first[:, c] = (resid_scale * stream_in[:, c].astype(F32)
+                       + jnp.dot(norm_in[...], wout[:, c], preferred_element_type=F32))
+    f = first[...]
+    mean = jnp.sum(f, axis=1, keepdims=True) * (1.0 / D)
+    var = jnp.sum(f * f, axis=1, keepdims=True) * (1.0 / D) - mean * mean
+    tok[mine, :] = ((f - mean) * lax.rsqrt(var + norm_eps) * gains[0:1, :]).astype(BF16)
+    tg = TpGather(tok.at[mine], tok, share, tk_s, tk_r, sp, tp)
+    tg.begin()
+    for n in range(10, 15):
+        ring.step(n)
+    ring.finish()
+
+    x, c = tp // 2, lax.rem(tp, 2)
+
+    def chip(d):
+        return lax.rem(x + d + 4, 4)
+
+    def chunk_rows(d):
+        return pl.ds(pl.multiple_of(chip(d) * 2 * share, 64), 2 * share)
+
+    order = (0, -1, 1, 2)
+    away = (1, -1, 2)
+
+    def compute(k):
+        chunk = tok[chunk_rows(order[k]), :]
+        for n in range(4):
+            hidden = jnp.maximum(jnp.dot(chunk, up[:, 256 * n : 256 * n + 256], preferred_element_type=F32), 0.0)
+            squares[:, 256 * n : 256 * n + 256] = (hidden * hidden).astype(BF16)
+        sq = squares[...]
+        for e in range(4):
+            for other in (True, False):
+                q = 2 * e + (1 - c if other else c)
+                w = down[pl.ds(pl.multiple_of(q * 256, 256), 256), :]
+                part = lax.dot_general(sq, w, (((1,), (1,)), ((), ())), preferred_element_type=F32)
+                if other:
+                    sib_out[k, e] = part.astype(BF16)
+                else:
+                    own_part[k % 2, e] = part
+        copy = copy_to(sib_out.at[k], sib_in.at[k], sb_s.at[k], sb_r.at[k], (sp, 2 * x + 1 - c))
+        copy.start()
+        return copy
+
+    def pass_on(k, copy):
+        copy.wait()
+        local[chunk_rows(order[k]), :] = own_part[k % 2, x] + sib_in[k, x].astype(F32)
+        for e, d in enumerate(away):
+            outgoing[k, e] = (own_part[k % 2, chip(d)] + sib_in[k, chip(d)].astype(F32)).astype(BF16)
+        for e, d in enumerate(away):
+            push = copy_to(outgoing.at[k, e], parts.at[e, chunk_rows(order[k])], rs_s.at[k, e], rs_r.at[k, e],
+                           (sp, 2 * chip(d) + c))
+            push.start()
+            sends.append(push)
+
+    tg.sibling(2)
+    copy0 = compute(0)
+    tg.relay()
+    tg.sibling(5)
+    copy1 = compute(1)
+    pass_on(0, copy0)
+    tg.sibling(6)
+    copy2 = compute(2)
+    pass_on(1, copy1)
+    tg.far()
+    tg.sibling(7)
+    copy3 = compute(3)
+    pass_on(2, copy2)
+    pass_on(3, copy3)
+    for k in range(4):
+        for e, d in enumerate(away):
+            r = parts.at[e, chunk_rows(order[k] - d)]
+            copy_to(r, r, rs_s.at[k, e], rs_r.at[k, e], (sp, 2 * chip(d) + c)).wait_recv()
+
+    lane_at = lax.broadcasted_iota(jnp.int32, (128, 128), 1)
+    for t in range(tiles):
+        r = pl.ds(128 * t, 128)
+        y = local[r, :] + resid_scale * tok[r, my_cols].astype(F32)
+        for e in range(3):
+            y += parts[e, r, :].astype(F32)
+        local[r, :] = y
+        one = jnp.sum(y, axis=1, keepdims=True)
+        two = jnp.sum(y * y, axis=1, keepdims=True)
+        pair = jnp.where(lane_at == 0, one, jnp.where(lane_at == 1, two, 0.0))
+        stat_out[:, 128 * t : 128 * t + 128] = jnp.transpose(pair)[0:8, :]
+    for d in range(1, n_tp):
+        push = copy_to(stat_out, stat_in.at[d - 1], st_s.at[d - 1], st_r.at[d - 1], (sp, peer(d)))
+        push.start()
+        sends.append(push)
+    for copy in sends + ring.sent + wo.sent + tg.sent:
+        copy.wait_send()
+    stats = stat_out[...]
+    for d in range(1, n_tp):
+        copy_to(stat_in.at[d - 1], stat_in.at[d - 1], st_s.at[d - 1], st_r.at[d - 1], (sp, peer(d))).wait_recv()
+        stats += stat_in[d - 1]
+    mean = stats[0:1] * (1.0 / D)
+    scale = lax.rsqrt(stats[1:2] * (1.0 / D) - mean * mean + norm_eps)
+    rowq[0:1, :] = mean
+    rowq[1:2, :] = scale
+    for t in range(tiles):
+        r = pl.ds(128 * t, 128)
+        both = jnp.transpose(rowq[:, 128 * t : 128 * t + 128])
+        out[r, :] = ((local[r, :] - both[:, 0:1]) * both[:, 1:2] * last_gain[...]).astype(BF16)
+
+
+def per_device(hv, em, rm, gate, step, sudden, document_index, rate, bias, tv, te, tr, gain,
+               out_weight, stream, first_gain, last_gain, up_in, down_in):
     rows = hv.shape[0]
     n_sp = lax.axis_size("sp")
     sp = lax.axis_index("sp")
@@ -238,11 +565,14 @@
     first = lax.dynamic_slice_in_dim(jnp.pad(grid[:, 0], REACH, constant_values=-1), sp + REACH + 1, REACH)
     mask = jnp.concatenate([(last == last[0]) & (last >= 0), (first == first[0]) & (first >= 0)]).astype(F32)
     taps = jnp.pad(jnp.concatenate([tv, te, tr], axis=1).astype(F32), ((0, 3), (0, 0)))
+    gains = jnp.broadcast_to(first_gain[None, :], (8, 256))
     vmem = pl.BlockSpec(memory_space=pltpu.VMEM)
+    dma = pltpu.SemaphoreType.DMA
+    share = rows // 8
     return pl.pallas_call(
-        mixer_kernel,
+        layer_kernel,
         out_shape=jax.ShapeDtypeStruct((rows, 256), BF16),
-        in_specs=[vmem] * 5 + [pl.BlockSpec(memory_space=pltpu.SMEM)] + [vmem] * 2,
+        in_specs=[vmem] * 5 + [pl.BlockSpec(memory_space=pltpu.SMEM)] + [vmem] * 8,
         out_specs=vmem,
         scratch_shapes=[
             pltpu.VMEM((16, 256), BF16), pltpu.VMEM((16, 128), BF16), pltpu.VMEM((16, 128), BF16),
@@ -256,62 +586,25 @@
             pltpu.VMEM((rows, 256), F32),
             pltpu.VMEM((STATE + 16, 256), BF16), pltpu.VMEM((STATE + 16, 256), BF16),
             pltpu.VMEM((REACH, STATE + 16, 256), BF16), pltpu.VMEM((REACH, STATE + 16, 256), BF16),
-            pltpu.SemaphoreType.DMA((6,)), pltpu.SemaphoreType.DMA((6,)),
-            pltpu.SemaphoreType.DMA((2 * REACH,)), pltpu.SemaphoreType.DMA((2 * REACH,)),
+            pltpu.VMEM((D, 1024), BF16), pltpu.VMEM((D, 1024), BF16), pltpu.VMEM((D, D), BF16),
+            pltpu.VMEM((rows, 256), BF16), pltpu.VMEM((share, D), BF16), pltpu.VMEM((share, D), BF16),
+            pltpu.VMEM((8, D), F32), pltpu.VMEM((share, D), F32), pltpu.VMEM((rows, D), BF16),
+            pltpu.VMEM((2 * share, 1024), BF16),
+            pltpu.VMEM((4, 4, 2 * share, 256), BF16), pltpu.VMEM((4, 4, 2 * share, 256), BF16),
+            pltpu.VMEM((2, 4, 2 * share, 256), F32), pltpu.VMEM((4, 3, 2 * share, 256), BF16),
+            pltpu.VMEM((3, rows, 256), BF16), pltpu.VMEM((8, rows), F32), pltpu.VMEM((7, 8, rows), F32),
+            dma((6,)), dma((6,)), dma((2 * REACH,)), dma((2 * REACH,)),
+            dma((2,)), dma((2,)), dma((2,)), dma((2,)), dma((2, 4, 4)), dma((2, 4, 4)),
+            dma((2, 4)), dma((2, 4)), dma((8, 2)), dma((8, 2)), dma((8, 2)), dma((8, 2)),
+            dma((8,)), dma((8,)), dma((8,)), dma((8,)), dma((3, 7)), dma((3, 7)),
+            dma((4,)), dma((4,)), dma((4, 3)), dma((4, 3)), dma((7,)), dma((7,)),
         ],
         compiler_params=pltpu.CompilerParams(
-            collective_id=0, has_side_effects=True, vmem_limit_bytes=40 * 1024 * 1024),
-        cost_estimate=pl.CostEstimate(flops=2_000_000_000, bytes_accessed=3_000_000, transcendentals=0),
-        name="mixer",
-    )(hv, em, rm, gate, per_token, mask, taps, gain[None, :])
-
-
-def cut_along(array, dim, count):
-    dims = array.shape
-    blocks = array.reshape(*dims[:dim], count, dims[dim] // count, *dims[dim + 1 :])
-    return jnp.moveaxis(blocks, dim, 0)
-
-
-def sent_and_summed(array, axis, dim):
-    blocks = cut_along(array, dim, lax.axis_size(axis))
-    arrived = lax.all_to_all(blocks, axis, split_axis=0, concat_axis=0, tiled=True)
-    return arrived.astype(jnp.float32).sum(axis=0)
-
-
-def norm_rows(residual, gain, width):
-    sums = lax.psum((jnp.sum(residual, axis=1), jnp.sum(residual * residual, axis=1)), "tp")
-    row_mean = sums[0] / width
-    row_var = sums[1] / width - row_mean * row_mean
-    return ((residual - row_mean[:, None]) * lax.rsqrt(row_var + norm_eps)[:, None] * gain).astype(
-        jnp.bfloat16
-    )
-
-
-def per_device(hv, em, rm, gate, step, sudden, document_index, rate, bias, tv, te, tr, gain,
-               mixer_output_weight, stream, mixer_norm_gain, channel_norm_gain, up, down):
-    normed = mixer(hv, em, rm, gate, step, sudden, document_index, rate, bias, tv, te, tr, gain)
-    partial_value = jnp.dot(normed, mixer_output_weight, preferred_element_type=jnp.float32)
-    mixer_sum = sent_and_summed(partial_value.astype(jnp.bfloat16), "tp", 1)
-    first_sum = resid_scale * stream.astype(jnp.float32) + mixer_sum
-    normed_one = norm_rows(first_sum, mixer_norm_gain, D)
-    up_full, down_full = (
-        lax.all_gather(up, "sp", axis=0, tiled=True),
-        lax.all_gather(down, "sp", axis=0, tiled=True),
-    )
-    hidden = jnp.dot(
-        lax.all_gather(normed_one, "tp", axis=1, tiled=True),
-        up_full,
-        preferred_element_type=jnp.float32,
-    )
-    squared = jnp.square(jax.nn.relu(hidden)).astype(jnp.bfloat16)
-    down_part = lax.dot_general(
-        squared, down_full, (((1,), (1,)), ((), ())), preferred_element_type=jnp.float32
-    )
-    down_sum = lax.psum_scatter(
-        down_part.astype(jnp.bfloat16), "tp", scatter_dimension=1, tiled=True
-    ).astype(jnp.float32)
-    second_sum = resid_scale * normed_one.astype(jnp.float32) + down_sum
-    return norm_rows(second_sum, channel_norm_gain, D)
+            collective_id=0, has_side_effects=True, vmem_limit_bytes=60 * 1024 * 1024),
+        cost_estimate=pl.CostEstimate(flops=9_000_000_000, bytes_accessed=8_000_000, transcendentals=0),
+        name="layer",
+    )(hv, em, rm, gate, per_token, mask, taps, gain[None, :], up_in, down_in, out_weight, stream, gains,
+      last_gain[None, :])
 
 
 SPECS = (

time: 287 us -> 135 us (0.47)
  waiting for transfers between devices: 129 us -> 0 us
  Pallas kernels: 40.4 us -> 123 us
  blocking collectives: 72.5 us -> 0 us
  between operations: 13.3 us -> 0.13 us
  matrix products: 12.9 us -> 0 us
  other arithmetic: 8.95 us -> 2.75 us
    all_gather x3 -> x0, waiting for transfers between devices: 90.7 us -> none  [the longest x1 54.4 us: per_device(): lax.all_gather(down, 'sp', axis=0, tiled=True)]
    pallas_call x1, Pallas kernels: 40.4 us -> 123 us  [per_device(): pl.pallas_call(layer_kernel, out_shape=jax.ShapeDtypeStruct((rows, 256),...]
    all_to_all x1 -> x0, blocking collectives: 43.8 us -> none  [sent_and_summed(): lax.all_to_all(blocks, axis, split_axis=0, concat_axis=0, tiled=True)]
    reduce_scatter x1 -> x0, waiting for transfers between devices: 36.7 us -> none  [per_device(): lax.psum_scatter(down_part.astype(jnp.bfloat16), 'tp', scatter_dimension=...]
    psum x2 -> x0, blocking collectives: 28.7 us -> none  [norm_rows(): lax.psum((jnp.sum(residual, axis=1), jnp.sum(residual * residual, axis=1)...]
    dot_general x2 -> x0, matrix products: 12.9 us -> none  [the longest x1 11.9 us: per_device(): lax.dot_general(squared, down_full, (((1,), (1,)), ((), ())), preferred_e...]
  transfers between devices with their start and end apart: 4 -> 0, of which waited for: 3 -> 0; matrix products, arithmetic and copies ran while one was open for 4% -> 0% of each run, Pallas kernels for 14% -> 0%
where the time goes in v2:
time: 135 us
  Pallas kernels  123 us (91%)
  local copies, waits for them, and re-layouts  8.81 us (7%)
  other arithmetic  2.75 us (2%)
    pallas_call x1, Pallas kernels, per_device(): pl.pallas_call(layer_kernel, out_shape=jax.ShapeDtypeStruct((rows, 256),...  123 us
    unnamed x19, local copies, waits for them, and re-layouts  3.28 us

profile of v2, /device:TPU:1, one launch (start us, length us, event | category | flops | bytes accessed | tf_op | source)
XLA Modules:
  0.0 134.7 jit_solution(4759812160316580891)
XLA Ops:
  0.0 0.0 copy-start.8
  0.0 0.0 copy-start.7
  0.0 0.7 copy-done.8
  0.7 0.0 copy-done.7
  0.7 0.8 fusion.20
  1.5 0.6 fusion.21
  2.1 0.6 broadcast_in_dim.48
  2.8 0.0 copy-start.6
  2.8 0.6 broadcast_in_dim.47
  3.4 0.0 copy-done.6
  3.5 0.0 copy-start.3
  3.5 0.0 copy-start.4
  3.5 0.0 copy-start.5
  3.5 0.6 broadcast_in_dim.51.gains_in
  4.1 0.1 copy-done.3
  4.1 0.0 copy-done.4
  4.2 0.0 copy-done.5
  4.2 0.6 fusion.19.taps
  4.8 0.1 fusion.22
  4.9 0.0 copy-start.1
  4.9 0.0 copy-start.2
  4.9 0.6 copy-done.1
  5.6 0.0 copy-done.2
  5.6 0.0 copy-start
  5.6 0.1 bitcast_add_fusion
  5.7 1.9 %concatenate.9.per_token = f32[24,768]{1,0:T(8,128)} concatenate(f32[4,768]{1,0:T(4,128)S(1)} %get-tuple-element.12, f32[4,768]{1,0:T(4,128)S(1)} %get-tuple-element.8, f32[4,768]{1,0:T(4,128)S(1)} %get-tuple-element.11, f32[4,768]{1,0:T(4,128)S(1)} %get-tuple-element.7, f32[1,768]{1,0:T(1,128)S(1)} %broadcast_in_dim.42, f32[1,768]{1,0:T(1,128)S(1)} %broadcast_in_dim.43, ...), dimensions={0} | concatenate | bytes 147456 | tf_op jit(solution)/shard_map/concatenate | solution.py:562
  7.6 0.0 copy-done
  7.6 0.2 slice_reduce_fusion.1
  7.8 0.1 pad_dynamic-slice_fusion.1
  7.9 0.6 slice.64
  8.6 0.1 rev.3
  8.7 0.6 compare_and_fusion.1
  9.3 0.6 add_convert_fusion.source_mask
  9.9 123.0 %layer.1 = bf16[768,256]{1,0:T(8,128)(2,1)} custom-call(bf16[768,256]{1,0:T(8,128)(2,1)} %hv.1, bf16[768,128]{1,0:T(8,128)(2,1)} %em.1, bf16[768,128]{1,0:T(8,128)(2,1)} %rm.1, bf16[768,256]{1,0:T(8,128)(2,1)} %gate.1, f32[24,768]{1,0:T(8,128)} %concatenate.9.per_token, f32[16]{0:T(128)} %add_convert_fusion.source_mask, f32[8,512]{1,0:T(8,128)} %fusion.19.taps, ...), custom_call_target="tpu_custom_call" | custom-call | flops 8999999488 | bytes 8000000 | tf_op jit(solution)/shard_map/layer/pallas_call | solution.py:572
  132.9 1.8 %copy.21 = bf16[768,256]{1,0:T(8,128)(2,1)} copy(bf16[768,256]{1,0:T(8,128)(2,1)} %layer.1) | data formatting | bytes 786432
  (9 shorter events, 0.1 us)
Async XLA Ops:
  0.0 0.7 copy-start.8
  0.0 0.7 copy-start.7
  2.8 0.7 copy-start.6
  3.5 0.7 copy-start.3
  3.5 0.7 copy-start.4
  3.5 0.7 copy-start.5
  4.9 0.7 copy-start.1
  4.9 0.7 copy-start.2
  5.6 2.0 %copy-start = (s32[24576]{0:T(1024)S(1)}, s32[24576]{0:T(1024)}, u32[]{:S(2)}) copy-start(s32[24576]{0:T(1024)} %param.25) | copy-start | bytes 294916

commit v3 on v2

--- a/solution.py
+++ b/solution.py
@@ -108,7 +108,7 @@
                     self.send(self.down.at[r], self.down.at[r], self.dh_s.at[k, m], self.dh_r.at[k, m],
                               self.dev(0, sign))
 
-    def step(self, n):
+    def up_step(self, n):
         s, part = divmod(n, 3)
         if part == 0:
             if s == 0:
@@ -117,11 +117,8 @@
                               self.dev(0, sign))
             else:
                 self.up_z(s - 1, 0, True)
-                self.down_z(s - 1, True)
             if s < 4:
                 self.up_z(s, 0, False)
-                self.down_z(s, False)
-            self.down_y(s)
         elif part == 1:
             if s == 0:
                 for m, sign in enumerate((1, -1)):
@@ -134,7 +131,6 @@
             if s < 4:
                 self.up_z(s, 1, False)
                 self.up_z(s, 3, False)
-            self.down_half(s, False)
         else:
             if s == 0:
                 for m, sign in enumerate((1, -1)):
@@ -144,6 +140,13 @@
             if s < 4:
                 self.up_z(s, 2, False)
 
+    def down_step(self, s):
+        if s > 0:
+            self.down_z(s - 1, True)
+        if s < 4:
+            self.down_z(s, False)
+        self.down_y(s)
+
     def finish(self):
         for s in range(5):
             self.down_half(s, True)
@@ -195,12 +198,13 @@
 
 
 def layer_kernel(
-    hv, em, rm, gate, per_token, source_mask, taps, gain, up_in, down_in, wout_in, stream, gains_in, last_gain, out,
+    hv, em, rm, gate, step_in, sudden_in, docs_in, rate, bias, tap_v, tap_e, tap_r, gain, up_in, down_in, wout_in,
+    stream, first_gain, last_gain, out,
     prev_v, prev_e, prev_r, next_v, next_e, next_r,
-    wide, rowq, cols, val, ent, ent32, rdo, weight, local,
-    msg0, msg1, got0, got1,
+    per_token, gains_in, wide, rowq, cols, val, ent, ent32, rdo, weight, local,
+    msg0, msg1, got0, got1, wmsg0, wmsg1, wgot0, wgot1, states,
     up, down, wout, norm_out, norm_in, stream_in, gains, first, tok, squares,
-    sib_out, sib_in, own_part, outgoing, parts, stat_out, stat_in,
+    sib_out, sib_in, own_part, outgoing, parts, relay, stat_out, stat_in,
     halo_send, halo_recv, state_send, state_recv,
     uy_s, uy_r, uh_s, uh_r, uz_s, uz_r, dz_s, dz_r, dy_s, dy_r, dh_s, dh_r,
     wo_s, wo_r, tk_s, tk_r, ex_s, ex_r, sb_s, sb_r, rs_s, rs_r, st_s, st_r,
@@ -218,6 +222,7 @@
     def peer(d):
         return lax.rem(tp + d + n_tp, n_tp)
 
+    gains_in[...] = jnp.broadcast_to(first_gain[...].reshape(1, 256), (8, 256))
     barrier = pltpu.get_barrier_semaphore()
     for d in range(1, REACH + 1):
         for s in (d, -d):
@@ -235,7 +240,8 @@
         copy.start()
     ring = WeightRing(up_in, down_in, up, down,
                       (uy_s, uy_r, uh_s, uh_r, uz_s, uz_r, dz_s, dz_r, dy_s, dy_r, dh_s, dh_r), sp, tp)
-    ring.step(0)
+    ring.down_step(0)
+    ring.up_step(0)
     wo = TpGather(wout_in, wout, 256, wo_s, wo_r, sp, tp)
     wo.begin()
 
@@ -269,6 +275,46 @@
     up[own_rows, :] = up_in[...]
     down[own_rows, :] = down_in[...]
     wout[pl.ds(pl.multiple_of(tp * 256, 256), 256), :] = wout_in[...]
+
+    raw = step_in[...].astype(F32)
+    sudden = sudden_in[...]
+
+    def eight(ref):
+        return jnp.concatenate([jnp.full((1, rows), ref[k, h], F32) for k in range(2) for h in range(4)], axis=0)
+
+    before_softplus = jnp.concatenate([raw, raw], axis=0) + eight(bias)
+    per_token[0:8, :] = jnp.maximum(before_softplus, 0.0) + jnp.log1p(jnp.exp(-jnp.abs(before_softplus)))
+    per_token[8:16, :] = -jnp.exp(eight(rate)) * per_token[0:8, :] + jnp.concatenate([sudden, sudden], axis=0)
+
+    def doc_at(row, lane_no):
+        return docs_in[pl.ds(row, 1), lane_no : lane_no + 1].astype(F32)
+
+    own_doc = jnp.concatenate([docs_in[pl.ds(tiles * sp + t, 1), :] for t in range(tiles)], axis=1).astype(F32)
+    own8 = jnp.broadcast_to(own_doc, (8, rows))
+    low_row, high_row = jnp.maximum(tiles * sp - 1, 0), jnp.minimum(tiles * sp + tiles, tiles * n_sp - 1)
+    prev_two, prev_one = (jnp.where(sp > 0, doc_at(low_row, k), -1.0) for k in (126, 127))
+    next_one, next_two = (jnp.where(sp < n_sp - 1, doc_at(high_row, k), -1.0) for k in (0, 1))
+    lane8 = lax.broadcasted_iota(jnp.int32, (8, rows), 1)
+    back_one = jnp.where(lane8 == 0, prev_one, pltpu.roll(own8, 1, 1))
+    back_two = jnp.where(lane8 == 0, prev_two, jnp.where(lane8 == 1, prev_one, pltpu.roll(own8, 2, 1)))
+    on_one = jnp.where(lane8 == rows - 1, next_one, pltpu.roll(own8, rows - 1, 1))
+    on_two = jnp.where(lane8 == rows - 1, next_two, jnp.where(lane8 == rows - 2, next_one, pltpu.roll(own8, rows - 2, 1)))
+    for k, row in enumerate((back_two, back_one, own8, on_one, on_two)):
+        per_token[16 + k : 17 + k, :] = row[0:1]
+    per_token[21:22, :] = jnp.broadcast_to(prev_one, (1, rows))
+    per_token[22:23, :] = jnp.broadcast_to(next_one, (1, rows))
+    per_token[23:24, :] = jnp.zeros((1, rows), F32)
+
+    def last_doc(d):
+        return doc_at(tiles * lax.rem(sp - d + n_sp, n_sp) + tiles - 1, 127)
+
+    def first_doc(d):
+        return doc_at(tiles * lax.rem(sp + d, n_sp), 0)
+
+    source_mask = []
+    for edge, room in ((last_doc, sp), (first_doc, n_sp - 1 - sp)):
+        for d, to in ((1, 0), (2, 0), (4, 1), (7, 1)):
+            source_mask.append(jnp.where((edge(d) == edge(to)) & (room >= d), 1.0, 0.0))
 
     dt = per_token[0:8, :]
     log_decay = per_token[8:16, :]
@@ -312,6 +358,8 @@
     wide[8 + rows : 16 + rows, 256:384] = next_e[0:8, :].astype(F32)
     wide[8 + rows : 16 + rows, 384:512] = next_r[0:8, :].astype(F32)
 
+    whole_taps = tap_v[...].astype(F32)
+    taps = (whole_taps[:, 0:128], whole_taps[:, 128:256], tap_e[...].astype(F32), tap_r[...].astype(F32))
     for t in range(tiles):
         lo = 128 * t
         masks = [jnp.broadcast_to(cols[lo : lo + 128, CM + o : CM + o + 1], (128, 128)) for o in range(5)]
@@ -321,7 +369,7 @@
                 part = wide[lo + 6 + o : lo + 134 + o, 128 * g : 128 * g + 128]
                 if o != 2:
                     part = part * masks[o]
-                acc = acc + taps[o : o + 1, 128 * g : 128 * g + 128] * part
+                acc = acc + taps[g][o : o + 1] * part
             act = acc * jax.nn.sigmoid(acc)
             if g < 2:
                 val[lo : lo + 128, 128 * g : 128 * g + 128] = act.astype(BF16)
@@ -331,8 +379,9 @@
             else:
                 rdo[lo : lo + 128, :] = act.astype(BF16)
 
-    ring.step(1)
-    ring.step(2)
+    ring.up_step(1)
+    ring.down_step(1)
+    ring.down_half(0, False)
     state0 = jnp.zeros((STATE, 256), F32)
     state1 = jnp.zeros((STATE, 256), F32)
     for t in range(tiles):
@@ -341,31 +390,34 @@
         v = val[r, :].astype(F32)
         state0 += jnp.dot(ent_t, (v * lanes_of(cols, r, W0)).astype(BF16), preferred_element_type=F32)
         state1 += jnp.dot(ent_t, (v * lanes_of(cols, r, W1)).astype(BF16), preferred_element_type=F32)
-    for msg, state, whole in ((msg0, state0, all0), (msg1, state1, all1)):
+    def fill(msg, state, passing):
         msg[0:STATE, :] = state.astype(BF16)
-        passing = head_lanes([jnp.exp(whole[h : h + 1, :]) for h in range(4)])
         coarse = passing.astype(BF16)
         fine = (passing - coarse.astype(F32)).astype(BF16)
         row = lax.broadcasted_iota(jnp.int32, (16, 256), 0)
         both = jnp.where(row == 0, coarse.astype(F32), jnp.where(row == 1, fine.astype(F32), 0.0))
         msg[STATE : STATE + 16, :] = both.astype(BF16)
 
+    def passing_of(msg):
+        tail = msg[STATE : STATE + 16, :].astype(F32)
+        return tail[0:1] + tail[1:2]
+
+    pass_own = [head_lanes([jnp.exp(whole[h : h + 1, :]) for h in range(4)]) for whole in (all0, all1)]
+    for m, (msg, state) in enumerate(((msg0, state0), (msg1, state1))):
+        states[m] = state
+        fill(msg, state, pass_own[m])
+
     for t in range(tiles):
         r = pl.ds(128 * t, 128)
         own_score = jnp.sum(rdo[r, :].astype(F32) * ent[r, :].astype(F32), axis=1, keepdims=True)
         local[r, :] = own_score * lanes_of(cols, r, DT0) * val[r, :].astype(F32)
 
-    state_sends = []
-    for d in range(1, REACH + 1):
+    near_sends = []
+    for k, d in enumerate((1, 2)):
         for m, (msg, got, step) in enumerate(((msg0, got0, d), (msg1, got1, -d))):
-            k = 2 * (d - 1) + m
-            state_sends.append(pltpu.make_async_remote_copy(
-                src_ref=msg, dst_ref=got.at[d - 1],
-                send_sem=state_send.at[k], recv_sem=state_recv.at[k],
-                device_id=at(step), device_id_type=MESH))
-    for copy in state_sends:
+            near_sends.append(copy_to(msg, got.at[k], state_send.at[2 * k + m], state_recv.at[2 * k + m], at(step)))
+    for copy in near_sends:
         copy.start()
-    ring.step(3)
 
     low_lane = lax.broadcasted_iota(jnp.int32, (128, 128), 1) < HEAD_DIM
 
@@ -398,21 +450,38 @@
         return 0
 
     lax.fori_loop(0, tiles // 2, tile_step, 0)
-    ring.step(4)
-    lax.fori_loop(tiles // 2, tiles, tile_step, 0)
-    ring.step(5)
-    ring.step(6)
-
-    for copy in state_sends:
+    ring.up_step(2)
+    for copy in near_sends:
+        copy.wait()
+    for m, (got, wmsg) in enumerate(((got0, wmsg0), (got1, wmsg1))):
+        through = [pass_own[m]]
+        for k in range(2):
+            through.append(through[k] * passing_of(got.at[k]))
+        window = states[m]
+        for k in range(2):
+            window += got[k, 0:STATE, :].astype(F32) * (through[k] * source_mask[4 * m + k])
+        fill(wmsg, window, through[2])
+    far_sends = []
+    lax.fori_loop(tiles // 2, tiles // 2 + 1, tile_step, 0)
+    for k, d in enumerate((1, 4, 7)):
+        for m, (wmsg, wgot, step) in enumerate(((wmsg0, wgot0, d), (wmsg1, wgot1, -d))):
+            n = 4 + 2 * k + m
+            far_sends.append(copy_to(wmsg, wgot.at[k], state_send.at[n], state_recv.at[n], at(step)))
+    for copy in far_sends:
+        copy.start()
+    lax.fori_loop(tiles // 2 + 1, tiles, tile_step, 0)
+    ring.up_step(3)
+    ring.down_step(2)
+    ring.down_half(1, False)
+    for copy in far_sends:
         copy.wait()
     carried = []
-    for m, got in enumerate((got0, got1)):
-        through = jnp.ones((1, 256), F32)
-        state = jnp.zeros((STATE, 256), F32)
-        for d in range(1, REACH + 1):
-            state = state + got[d - 1, 0:STATE, :].astype(F32) * (through * source_mask[REACH * m + d - 1])
-            tail = got[d - 1, STATE : STATE + 16, :].astype(F32)
-            through = through * (tail[0:1] + tail[1:2])
+    for m, wgot in enumerate((wgot0, wgot1)):
+        once = passing_of(wgot.at[0])
+        twice = once * passing_of(wgot.at[1])
+        state = (wgot[0, 0:STATE, :].astype(F32)
+                 + wgot[1, 0:STATE, :].astype(F32) * (once * source_mask[4 * m + 2])
+                 + wgot[2, 0:STATE, :].astype(F32) * (twice * source_mask[4 * m + 3]))
         carried.append(state.astype(BF16))
 
     for t in range(tiles):
@@ -424,17 +493,23 @@
         z = gate[r, :].astype(F32)
         y = y * (z * jax.nn.sigmoid(z))
         y = y * lax.rsqrt(jnp.mean(y * y, axis=1, keepdims=True) + norm_eps)
-        norm_out[r, :] = (y * gain[...]).astype(BF16)
+        norm_out[r, :] = (y * gain[...].reshape(1, 256)).astype(BF16)
 
     norm_in[:, my_cols] = norm_out[mine, :]
     sends += exchange(2, token_rows(norm_out), norm_in)
-    ring.step(7)
-    ring.step(8)
+    ring.up_step(4)
+    ring.down_step(3)
     wo.relay()
+    ring.up_step(5)
+    ring.up_step(6)
+    ring.down_half(2, False)
+    ring.down_step(4)
+    ring.up_step(7)
+    ring.up_step(8)
+    ring.down_half(3, False)
     exchanged(0, stream_in)
     exchanged(1, gains)
     exchanged(2, norm_in)
-    ring.step(9)
     wo.far()
     for k in (2, 5, 6, 7):
         wo.sibling(k)
@@ -448,23 +523,29 @@
     tok[mine, :] = ((f - mean) * lax.rsqrt(var + norm_eps) * gains[0:1, :]).astype(BF16)
     tg = TpGather(tok.at[mine], tok, share, tk_s, tk_r, sp, tp)
     tg.begin()
-    for n in range(10, 15):
-        ring.step(n)
+    ring.up_step(9)
+    ring.down_half(4, False)
+    ring.up_step(10)
+    tg.relay()
+    ring.up_step(11)
+    tg.far()
+    ring.up_step(12)
+    ring.up_step(13)
+    ring.up_step(14)
     ring.finish()
+    for k in (2, 5, 6, 7):
+        tg.sibling(k)
 
     x, c = tp // 2, lax.rem(tp, 2)
 
     def chip(d):
         return lax.rem(x + d + 4, 4)
 
-    def chunk_rows(d):
-        return pl.ds(pl.multiple_of(chip(d) * 2 * share, 64), 2 * share)
-
-    order = (0, -1, 1, 2)
-    away = (1, -1, 2)
+    def chunk_rows(k):
+        return pl.ds(2 * share * k, 2 * share)
 
     def compute(k):
-        chunk = tok[chunk_rows(order[k]), :]
+        chunk = tok[chunk_rows(k), :]
         for n in range(4):
             hidden = jnp.maximum(jnp.dot(chunk, up[:, 256 * n : 256 * n + 256], preferred_element_type=F32), 0.0)
             squares[:, 256 * n : 256 * n + 256] = (hidden * hidden).astype(BF16)
@@ -477,46 +558,62 @@
                 if other:
                     sib_out[k, e] = part.astype(BF16)
                 else:
-                    own_part[k % 2, e] = part
+                    own_part[k % 3, e] = part
         copy = copy_to(sib_out.at[k], sib_in.at[k], sb_s.at[k], sb_r.at[k], (sp, 2 * x + 1 - c))
         copy.start()
         return copy
 
+    def push(src, dst, k, e, d):
+        copy = copy_to(src, dst, rs_s.at[k, e], rs_r.at[k, e], (sp, 2 * chip(d) + c))
+        copy.start()
+        sends.append(copy)
+
     def pass_on(k, copy):
         copy.wait()
-        local[chunk_rows(order[k]), :] = own_part[k % 2, x] + sib_in[k, x].astype(F32)
-        for e, d in enumerate(away):
-            outgoing[k, e] = (own_part[k % 2, chip(d)] + sib_in[k, chip(d)].astype(F32)).astype(BF16)
-        for e, d in enumerate(away):
-            push = copy_to(outgoing.at[k, e], parts.at[e, chunk_rows(order[k])], rs_s.at[k, e], rs_r.at[k, e],
-                           (sp, 2 * chip(d) + c))
-            push.start()
-            sends.append(push)
-
-    tg.sibling(2)
+        outgoing[k, 2] = (own_part[k % 3, chip(2)] + sib_in[k, chip(2)].astype(F32)).astype(BF16)
+        local[chunk_rows(k), :] = own_part[k % 3, x] + sib_in[k, x].astype(F32)
+        for e, d in enumerate((1, -1)):
+            half = pl.ds(share * e, share)
+            push(outgoing.at[k, 2, half], relay.at[k, e], k, 2 + e, d)
+
+    def push_near(k):
+        for e, d in enumerate((1, -1)):
+            copy_to(relay.at[k, e], relay.at[k, e], rs_s.at[k, 2 + e], rs_r.at[k, 2 + e], (sp, 2 * chip(d) + c)).wait_recv()
+            half, rest = pl.ds(share * e, share), pl.ds(share * (1 - e), share)
+            total = own_part[k % 3, chip(d), half] + sib_in[k, chip(d), half].astype(F32)
+            outgoing[k, e, half] = (total + relay[k, e].astype(F32)).astype(BF16)
+            total = own_part[k % 3, chip(d), rest] + sib_in[k, chip(d), rest].astype(F32)
+            outgoing[k, e, rest] = total.astype(BF16)
+        for e, d in enumerate((1, -1)):
+            push(outgoing.at[k, e], parts.at[e, chunk_rows(k)], k, e, d)
+
     copy0 = compute(0)
-    tg.relay()
-    tg.sibling(5)
     copy1 = compute(1)
     pass_on(0, copy0)
-    tg.sibling(6)
     copy2 = compute(2)
     pass_on(1, copy1)
-    tg.far()
-    tg.sibling(7)
+    push_near(0)
     copy3 = compute(3)
     pass_on(2, copy2)
+    push_near(1)
     pass_on(3, copy3)
-    for k in range(4):
-        for e, d in enumerate(away):
-            r = parts.at[e, chunk_rows(order[k] - d)]
+    push_near(2)
+    push_near(3)
+    def parts_arrived(k):
+        for e, d in enumerate((1, -1)):
+            r = parts.at[e, chunk_rows(k)]
             copy_to(r, r, rs_s.at[k, e], rs_r.at[k, e], (sp, 2 * chip(d) + c)).wait_recv()
+
+    parts_arrived(0)
+    parts_arrived(1)
+    parts_arrived(2)
+    parts_arrived(3)
 
     lane_at = lax.broadcasted_iota(jnp.int32, (128, 128), 1)
     for t in range(tiles):
         r = pl.ds(128 * t, 128)
         y = local[r, :] + resid_scale * tok[r, my_cols].astype(F32)
-        for e in range(3):
+        for e in range(2):
             y += parts[e, r, :].astype(F32)
         local[r, :] = y
         one = jnp.sum(y, axis=1, keepdims=True)
@@ -524,14 +621,21 @@
         pair = jnp.where(lane_at == 0, one, jnp.where(lane_at == 1, two, 0.0))
         stat_out[:, 128 * t : 128 * t + 128] = jnp.transpose(pair)[0:8, :]
     for d in range(1, n_tp):
-        push = copy_to(stat_out, stat_in.at[d - 1], st_s.at[d - 1], st_r.at[d - 1], (sp, peer(d)))
-        push.start()
-        sends.append(push)
-    for copy in sends + ring.sent + wo.sent + tg.sent:
-        copy.wait_send()
+        copy = copy_to(stat_out, stat_in.at[d - 1], st_s.at[d - 1], st_r.at[d - 1], (sp, peer(d)))
+        copy.start()
+        sends.append(copy)
+
+    def stats_arrived():
+        for d in range(1, n_tp):
+            copy_to(stat_in.at[d - 1], stat_in.at[d - 1], st_s.at[d - 1], st_r.at[d - 1], (sp, peer(d))).wait_recv()
+
+    def all_sent():
+        for copy in sends + ring.sent + wo.sent + tg.sent:
+            copy.wait_send()
+
+    stats_arrived()
     stats = stat_out[...]
     for d in range(1, n_tp):
-        copy_to(stat_in.at[d - 1], stat_in.at[d - 1], st_s.at[d - 1], st_r.at[d - 1], (sp, peer(d))).wait_recv()
         stats += stat_in[d - 1]
     mean = stats[0:1] * (1.0 / D)
     scale = lax.rsqrt(stats[1:2] * (1.0 / D) - mean * mean + norm_eps)
@@ -540,43 +644,26 @@
     for t in range(tiles):
         r = pl.ds(128 * t, 128)
         both = jnp.transpose(rowq[:, 128 * t : 128 * t + 128])
-        out[r, :] = ((local[r, :] - both[:, 0:1]) * both[:, 1:2] * last_gain[...]).astype(BF16)
+        out[r, :] = ((local[r, :] - both[:, 0:1]) * both[:, 1:2] * last_gain[...].reshape(1, 256)).astype(BF16)
+    all_sent()
 
 
 def per_device(hv, em, rm, gate, step, sudden, document_index, rate, bias, tv, te, tr, gain,
                out_weight, stream, first_gain, last_gain, up_in, down_in):
     rows = hv.shape[0]
-    n_sp = lax.axis_size("sp")
-    sp = lax.axis_index("sp")
-    raw, sud = step.astype(F32).T, sudden.T
-    dts, lds = [], []
-    for k in range(2):
-        dt = jax.nn.softplus(raw + bias[k][:, None])
-        dts.append(dt)
-        lds.append(-jnp.exp(rate[k])[:, None] * dt + sud)
-    pad = jnp.pad(document_index, 3, constant_values=-1).astype(F32)
-    window = lax.dynamic_slice_in_dim(pad, sp * rows, rows + 6)
-    shifted = [window[1 + o : 1 + o + rows][None] for o in range(5)]
-    before = jnp.broadcast_to(window[2:3], (1, rows))
-    after = jnp.broadcast_to(window[rows + 3 : rows + 4], (1, rows))
-    per_token = jnp.concatenate(dts + lds + shifted + [before, after, jnp.zeros((1, rows), F32)], axis=0)
-    grid = document_index.reshape(n_sp, rows)
-    last = lax.dynamic_slice_in_dim(jnp.pad(grid[:, rows - 1], REACH, constant_values=-1), sp, REACH)[::-1]
-    first = lax.dynamic_slice_in_dim(jnp.pad(grid[:, 0], REACH, constant_values=-1), sp + REACH + 1, REACH)
-    mask = jnp.concatenate([(last == last[0]) & (last >= 0), (first == first[0]) & (first >= 0)]).astype(F32)
-    taps = jnp.pad(jnp.concatenate([tv, te, tr], axis=1).astype(F32), ((0, 3), (0, 0)))
-    gains = jnp.broadcast_to(first_gain[None, :], (8, 256))
+    docs = document_index.reshape(-1, 128)
     vmem = pl.BlockSpec(memory_space=pltpu.VMEM)
     dma = pltpu.SemaphoreType.DMA
     share = rows // 8
     return pl.pallas_call(
         layer_kernel,
         out_shape=jax.ShapeDtypeStruct((rows, 256), BF16),
-        in_specs=[vmem] * 5 + [pl.BlockSpec(memory_space=pltpu.SMEM)] + [vmem] * 8,
+        in_specs=[vmem] * 7 + [pl.BlockSpec(memory_space=pltpu.SMEM)] * 2 + [vmem] * 10,
         out_specs=vmem,
         scratch_shapes=[
             pltpu.VMEM((16, 256), BF16), pltpu.VMEM((16, 128), BF16), pltpu.VMEM((16, 128), BF16),
             pltpu.VMEM((16, 256), BF16), pltpu.VMEM((16, 128), BF16), pltpu.VMEM((16, 128), BF16),
+            pltpu.VMEM((24, rows), F32), pltpu.VMEM((8, 256), F32),
             pltpu.VMEM((rows + 16, 512), F32),
             pltpu.VMEM((128, rows), F32),
             pltpu.VMEM((rows, 128), F32),
@@ -585,26 +672,29 @@
             pltpu.VMEM((2, 128, rows), F32),
             pltpu.VMEM((rows, 256), F32),
             pltpu.VMEM((STATE + 16, 256), BF16), pltpu.VMEM((STATE + 16, 256), BF16),
-            pltpu.VMEM((REACH, STATE + 16, 256), BF16), pltpu.VMEM((REACH, STATE + 16, 256), BF16),
+            pltpu.VMEM((2, STATE + 16, 256), BF16), pltpu.VMEM((2, STATE + 16, 256), BF16),
+            pltpu.VMEM((STATE + 16, 256), BF16), pltpu.VMEM((STATE + 16, 256), BF16),
+            pltpu.VMEM((3, STATE + 16, 256), BF16), pltpu.VMEM((3, STATE + 16, 256), BF16),
+            pltpu.VMEM((2, STATE, 256), F32),
             pltpu.VMEM((D, 1024), BF16), pltpu.VMEM((D, 1024), BF16), pltpu.VMEM((D, D), BF16),
             pltpu.VMEM((rows, 256), BF16), pltpu.VMEM((share, D), BF16), pltpu.VMEM((share, D), BF16),
             pltpu.VMEM((8, D), F32), pltpu.VMEM((share, D), F32), pltpu.VMEM((rows, D), BF16),
             pltpu.VMEM((2 * share, 1024), BF16),
             pltpu.VMEM((4, 4, 2 * share, 256), BF16), pltpu.VMEM((4, 4, 2 * share, 256), BF16),
-            pltpu.VMEM((2, 4, 2 * share, 256), F32), pltpu.VMEM((4, 3, 2 * share, 256), BF16),
-            pltpu.VMEM((3, rows, 256), BF16), pltpu.VMEM((8, rows), F32), pltpu.VMEM((7, 8, rows), F32),
-            dma((6,)), dma((6,)), dma((2 * REACH,)), dma((2 * REACH,)),
+            pltpu.VMEM((3, 4, 2 * share, 256), F32), pltpu.VMEM((4, 3, 2 * share, 256), BF16),
+            pltpu.VMEM((2, rows, 256), BF16), pltpu.VMEM((4, 2, share, 256), BF16), pltpu.VMEM((8, rows), F32), pltpu.VMEM((7, 8, rows), F32),
+            dma((6,)), dma((6,)), dma((10,)), dma((10,)),
             dma((2,)), dma((2,)), dma((2,)), dma((2,)), dma((2, 4, 4)), dma((2, 4, 4)),
             dma((2, 4)), dma((2, 4)), dma((8, 2)), dma((8, 2)), dma((8, 2)), dma((8, 2)),
             dma((8,)), dma((8,)), dma((8,)), dma((8,)), dma((3, 7)), dma((3, 7)),
-            dma((4,)), dma((4,)), dma((4, 3)), dma((4, 3)), dma((7,)), dma((7,)),
+            dma((4,)), dma((4,)), dma((4, 4)), dma((4, 4)), dma((7,)), dma((7,)),
         ],
         compiler_params=pltpu.CompilerParams(
             collective_id=0, has_side_effects=True, vmem_limit_bytes=60 * 1024 * 1024),
         cost_estimate=pl.CostEstimate(flops=9_000_000_000, bytes_accessed=8_000_000, transcendentals=0),
         name="layer",
-    )(hv, em, rm, gate, per_token, mask, taps, gain[None, :], up_in, down_in, out_weight, stream, gains,
-      last_gain[None, :])
+    )(hv, em, rm, gate, step.T, sudden.T, docs, rate, bias, tv, te, tr, gain, up_in, down_in, out_weight, stream,
+      first_gain, last_gain)
 
 
 SPECS = (

time: 135 us -> 113 us (0.84)
  Pallas kernels: 123 us -> 111 us
  local copies, waits for them, and re-layouts: 8.81 us -> 1.77 us
  other arithmetic: 2.75 us -> 0 us
    pallas_call x1, Pallas kernels: 123 us -> 111 us  [per_device(): pl.pallas_call(layer_kernel, out_shape=jax.ShapeDtypeStruct((rows, 256),...]
    concatenate x1 -> x0, local copies, waits for them, and re-layouts: 1.9 us -> none  [per_device(): jnp.concatenate(dts + lds + shifted + [before, after, jnp.zeros((1, rows)...]
    broadcast_in_dim x9 -> x0, local copies, waits for them, and re-layouts: 1.9 us -> none  [the longest x1 0.65 us: per_device(): after = jnp.broadcast_to(window[rows + 3:rows + 4], (1, rows))]
    slice x4 -> x0, local copies, waits for them, and re-layouts: 1.52 us -> none  [the longest x1 0.64 us: per_device(): after = jnp.broadcast_to(window[rows + 3:rows + 4], (1, rows))]
    unnamed x19 -> x1, local copies, waits for them, and re-layouts: 3.28 us -> 1.77 us
    convert_element_type x2 -> x0, other arithmetic: 1.36 us -> none  [the longest x1 0.78 us: per_device(): pad = jnp.pad(document_index, 3, constant_values=-1).astype(F32)]
where the time goes in v3:
time: 113 us; the launch traced here: 112 us
  Pallas kernels  111 us (98%)
  local copies, waits for them, and re-layouts  1.77 us (2%)
    pallas_call x1, Pallas kernels, per_device(): pl.pallas_call(layer_kernel, out_shape=jax.ShapeDtypeStruct((rows, 256),...  111 us

profile of v3, /device:TPU:1, one launch (start us, length us, event | category | flops | bytes accessed | tf_op | source)
XLA Modules:
  0.0 112.5 jit_solution(11059696745143722868)
XLA Ops:
  0.0 110.7 %layer.1 = bf16[768,256]{1,0:T(8,128)(2,1)} custom-call(bf16[768,256]{1,0:T(8,128)(2,1)} %hv.1, bf16[768,128]{1,0:T(8,128)(2,1)} %em.1, bf16[768,128]{1,0:T(8,128)(2,1)} %rm.1, bf16[768,256]{1,0:T(8,128)(2,1)} %gate.1, bf16[4,768]{1,0:T(4,128)(2,1)} %bitcast.5, f32[4,768]{1,0:T(4,128)} %bitcast.4, s32[192,128]{1,0:T(8,128)} %bitcast.3, f32[2,4]{1,0:T(2,128)} %rate.1, ...), custom_call_target="tpu_custom_call" | custom-call | flops 8999999488 | bytes 8000000 | tf_op jit(solution)/shard_map/layer/pallas_call | solution.py:658
  110.7 1.8 %copy.21 = bf16[768,256]{1,0:T(8,128)(2,1)} copy(bf16[768,256]{1,0:T(8,128)(2,1)} %layer.1) | data formatting | bytes 786432

commit v4 on v3

--- a/solution.py
+++ b/solution.py
@@ -198,16 +198,17 @@
 
 
 def layer_kernel(
-    hv, em, rm, gate, step_in, sudden_in, docs_in, rate, bias, tap_v, tap_e, tap_r, gain, up_in, down_in, wout_in,
-    stream, first_gain, last_gain, out,
+    hv_any, em_any, rm_any, gate_any, stream_any, wout_any, up_any, down_any,
+    step_in, sudden_in, docs_in, rate, bias, tap_v, tap_e, tap_r, gain, first_gain, last_gain, out,
+    hv, em, rm, gate, stream, wout_in,
     prev_v, prev_e, prev_r, next_v, next_e, next_r,
     per_token, gains_in, wide, rowq, cols, val, ent, ent32, rdo, weight, local,
     msg0, msg1, got0, got1, wmsg0, wmsg1, wgot0, wgot1, states,
-    up, down, wout, norm_out, norm_in, stream_in, gains, first, tok, squares,
+    up, down, norm_out, mix_sib, mix_got, mix_own, mix_far, mix_near, mix_relay, mix_in, stream_in, gains, first, tok, squares,
     sib_out, sib_in, own_part, outgoing, parts, relay, stat_out, stat_in,
-    halo_send, halo_recv, state_send, state_recv,
+    pull, halo_send, halo_recv, state_send, state_recv,
     uy_s, uy_r, uh_s, uh_r, uz_s, uz_r, dz_s, dz_r, dy_s, dy_r, dh_s, dh_r,
-    wo_s, wo_r, tk_s, tk_r, ex_s, ex_r, sb_s, sb_r, rs_s, rs_r, st_s, st_r,
+    mx_s, mx_r, tk_s, tk_r, ex_s, ex_r, sb_s, sb_r, rs_s, rs_r, st_s, st_r,
 ):
     sp, tp = lax.axis_index("sp"), lax.axis_index("tp")
     n_sp = lax.axis_size("sp")
@@ -222,14 +223,23 @@
     def peer(d):
         return lax.rem(tp + d + n_tp, n_tp)
 
+    own_rows = pl.ds(pl.multiple_of(sp * 64, 64), 64)
+    up_in, down_in = up.at[own_rows], down.at[own_rows]
+    barrier = pltpu.get_barrier_semaphore()
     gains_in[...] = jnp.broadcast_to(first_gain[...].reshape(1, 256), (8, 256))
-    barrier = pltpu.get_barrier_semaphore()
     for d in range(1, REACH + 1):
         for s in (d, -d):
             pl.semaphore_signal(barrier, inc=1, device_id=at(s), device_id_type=MESH)
     for d in range(1, n_tp):
         pl.semaphore_signal(barrier, inc=1, device_id=(sp, peer(d)), device_id_type=MESH)
+    pulls = [pltpu.make_async_copy(src, dst, pull.at[k]) for k, (src, dst) in enumerate((
+        (hv_any, hv), (em_any, em), (rm_any, rm), (up_any, up_in), (down_any, down_in), (stream_any, stream),
+        (gate_any, gate), (wout_any, wout_in)))]
+    for copy in pulls:
+        copy.start()
     pl.semaphore_wait(barrier, 2 * REACH + n_tp - 1)
+    for copy in pulls:
+        copy.wait()
 
     halos = []
     for k, (src, low, high) in enumerate(((hv, prev_v, next_v), (em, prev_e, next_e), (rm, prev_r, next_r))):
@@ -242,8 +252,6 @@
                       (uy_s, uy_r, uh_s, uh_r, uz_s, uz_r, dz_s, dz_r, dy_s, dy_r, dh_s, dh_r), sp, tp)
     ring.down_step(0)
     ring.up_step(0)
-    wo = TpGather(wout_in, wout, 256, wo_s, wo_r, sp, tp)
-    wo.begin()
 
     def my_lanes(ref, q):
         return ref.at[:, pl.ds(pl.multiple_of(q * 256, 256), 256)]
@@ -269,12 +277,8 @@
     sends += exchange(1, lambda q: gains_in, gains)
     mine = pl.ds(pl.multiple_of(tp * share, 16), share)
     my_cols = pl.ds(pl.multiple_of(tp * 256, 256), 256)
-    own_rows = pl.ds(pl.multiple_of(sp * 64, 64), 64)
     stream_in[:, my_cols] = stream[mine, :]
     gains[:, my_cols] = gains_in[...]
-    up[own_rows, :] = up_in[...]
-    down[own_rows, :] = down_in[...]
-    wout[pl.ds(pl.multiple_of(tp * 256, 256), 256), :] = wout_in[...]
 
     raw = step_in[...].astype(F32)
     sudden = sudden_in[...]
@@ -379,9 +383,6 @@
             else:
                 rdo[lo : lo + 128, :] = act.astype(BF16)
 
-    ring.up_step(1)
-    ring.down_step(1)
-    ring.down_half(0, False)
     state0 = jnp.zeros((STATE, 256), F32)
     state1 = jnp.zeros((STATE, 256), F32)
     for t in range(tiles):
@@ -418,6 +419,9 @@
             near_sends.append(copy_to(msg, got.at[k], state_send.at[2 * k + m], state_recv.at[2 * k + m], at(step)))
     for copy in near_sends:
         copy.start()
+    ring.down_step(1)
+    ring.up_step(1)
+    ring.down_half(0, False)
 
     low_lane = lax.broadcasted_iota(jnp.int32, (128, 128), 1) < HEAD_DIM
 
@@ -450,7 +454,6 @@
         return 0
 
     lax.fori_loop(0, tiles // 2, tile_step, 0)
-    ring.up_step(2)
     for copy in near_sends:
         copy.wait()
     for m, (got, wmsg) in enumerate(((got0, wmsg0), (got1, wmsg1))):
@@ -470,11 +473,12 @@
     for copy in far_sends:
         copy.start()
     lax.fori_loop(tiles // 2 + 1, tiles, tile_step, 0)
+    ring.down_step(2)
     ring.up_step(3)
-    ring.down_step(2)
     ring.down_half(1, False)
     for copy in far_sends:
         copy.wait()
+    ring.up_step(2)
     carried = []
     for m, wgot in enumerate((wgot0, wgot1)):
         once = passing_of(wgot.at[0])
@@ -495,38 +499,91 @@
         y = y * lax.rsqrt(jnp.mean(y * y, axis=1, keepdims=True) + norm_eps)
         norm_out[r, :] = (y * gain[...].reshape(1, 256)).astype(BF16)
 
-    norm_in[:, my_cols] = norm_out[mine, :]
-    sends += exchange(2, token_rows(norm_out), norm_in)
+    x, c = tp // 2, lax.rem(tp, 2)
+    half_share = share // 2
+
+    def chip(d):
+        return lax.rem(x + d + 4, 4)
+
+    def project(k, d):
+        for other in (True, False):
+            q = 2 * chip(d) + (1 - c if other else c)
+            part = jnp.dot(norm_out[pl.ds(pl.multiple_of(q * share, 16), share), :], wout_in[...],
+                           preferred_element_type=F32)
+            if other:
+                mix_sib[k] = part.astype(BF16)
+            else:
+                mix_own[k] = part
+        copy = copy_to(mix_sib.at[k], mix_got.at[k], mx_s.at[k], mx_r.at[k], (sp, 2 * x + 1 - c))
+        copy.start()
+        return copy
+
+    def mix_push(src, dst, n, d):
+        copy = copy_to(src, dst, mx_s.at[n], mx_r.at[n], (sp, 2 * chip(d) + c))
+        copy.start()
+        sends.append(copy)
+
+    def mix_arrived(dst, n):
+        copy_to(dst, dst, mx_s.at[n], mx_r.at[n], (sp, 2 * x + 1 - c)).wait_recv()
+
+    def mix_far_out():
+        crossing[0].wait()
+        mix_far[...] = (mix_own[0] + mix_got[0].astype(F32)).astype(BF16)
+        for e, d in enumerate((1, -1)):
+            mix_push(mix_far.at[pl.ds(half_share * e, half_share)], mix_relay.at[e], 4 + e, d)
+
+    def mix_near_rest():
+        for e, d in enumerate((1, -1)):
+            crossing[1 + e].wait()
+            rest = pl.ds(half_share * (1 - e), half_share)
+            mix_near[e, rest] = (mix_own[1 + e, rest] + mix_got[1 + e, rest].astype(F32)).astype(BF16)
+            mix_push(mix_near.at[e, rest], mix_in.at[e, rest], 6 + e, d)
+        crossing[3].wait()
+
+    def mix_near_last():
+        for e, d in enumerate((1, -1)):
+            mix_arrived(mix_relay.at[e], 4 + e)
+            half = pl.ds(half_share * e, half_share)
+            total = mix_own[1 + e, half] + mix_got[1 + e, half].astype(F32) + mix_relay[e].astype(F32)
+            mix_near[e, half] = total.astype(BF16)
+            mix_push(mix_near.at[e, half], mix_in.at[e, half], 8 + e, d)
+
+    def mix_finish():
+        for e in range(2):
+            mix_arrived(mix_in.at[e, pl.ds(half_share * (1 - e), half_share)], 6 + e)
+            mix_arrived(mix_in.at[e, pl.ds(half_share * e, half_share)], 8 + e)
+        first[...] = (resid_scale * stream_in[...].astype(F32) + mix_own[3] + mix_got[3].astype(F32)
+                      + mix_in[0].astype(F32) + mix_in[1].astype(F32))
+
+    crossing = [project(0, 2)]
+    crossing.append(project(1, 1))
+    mix_far_out()
+    crossing.append(project(2, -1))
+    crossing.append(project(3, 0))
+    mix_near_rest()
     ring.up_step(4)
+    mix_near_last()
     ring.down_step(3)
-    wo.relay()
     ring.up_step(5)
     ring.up_step(6)
     ring.down_half(2, False)
-    ring.down_step(4)
-    ring.up_step(7)
-    ring.up_step(8)
-    ring.down_half(3, False)
     exchanged(0, stream_in)
     exchanged(1, gains)
-    exchanged(2, norm_in)
-    wo.far()
-    for k in (2, 5, 6, 7):
-        wo.sibling(k)
-    for n in range(4):
-        c = pl.ds(512 * n, 512)
-        first[:, c] = (resid_scale * stream_in[:, c].astype(F32)
-                       + jnp.dot(norm_in[...], wout[:, c], preferred_element_type=F32))
+    mix_finish()
     f = first[...]
     mean = jnp.sum(f, axis=1, keepdims=True) * (1.0 / D)
     var = jnp.sum(f * f, axis=1, keepdims=True) * (1.0 / D) - mean * mean
     tok[mine, :] = ((f - mean) * lax.rsqrt(var + norm_eps) * gains[0:1, :]).astype(BF16)
     tg = TpGather(tok.at[mine], tok, share, tk_s, tk_r, sp, tp)
     tg.begin()
+    ring.down_step(4)
+    ring.up_step(7)
+    ring.up_step(8)
+    ring.down_half(3, False)
     ring.up_step(9)
+    tg.relay()
     ring.down_half(4, False)
     ring.up_step(10)
-    tg.relay()
     ring.up_step(11)
     tg.far()
     ring.up_step(12)
@@ -536,115 +593,133 @@
     for k in (2, 5, 6, 7):
         tg.sibling(k)
 
-    x, c = tp // 2, lax.rem(tp, 2)
-
-    def chip(d):
-        return lax.rem(x + d + 4, 4)
-
     def chunk_rows(k):
         return pl.ds(2 * share * k, 2 * share)
 
-    def compute(k):
+    def hidden(k):
         chunk = tok[chunk_rows(k), :]
         for n in range(4):
-            hidden = jnp.maximum(jnp.dot(chunk, up[:, 256 * n : 256 * n + 256], preferred_element_type=F32), 0.0)
-            squares[:, 256 * n : 256 * n + 256] = (hidden * hidden).astype(BF16)
+            h = jnp.maximum(jnp.dot(chunk, up[:, 256 * n : 256 * n + 256], preferred_element_type=F32), 0.0)
+            squares[:, 256 * n : 256 * n + 256] = (h * h).astype(BF16)
+
+    def compute(k):
         sq = squares[...]
-        for e in range(4):
+        for n, d in enumerate((2, 1, -1, 0)):
             for other in (True, False):
-                q = 2 * e + (1 - c if other else c)
+                q = 2 * chip(d) + (1 - c if other else c)
                 w = down[pl.ds(pl.multiple_of(q * 256, 256), 256), :]
                 part = lax.dot_general(sq, w, (((1,), (1,)), ((), ())), preferred_element_type=F32)
                 if other:
-                    sib_out[k, e] = part.astype(BF16)
+                    sib_out[k, n] = part.astype(BF16)
                 else:
-                    own_part[k % 3, e] = part
-        copy = copy_to(sib_out.at[k], sib_in.at[k], sb_s.at[k], sb_r.at[k], (sp, 2 * x + 1 - c))
-        copy.start()
-        return copy
+                    own_part[k % 3, n] = part
+        crossing = []
+        for n, r in enumerate((pl.ds(0, 1), pl.ds(1, 3))):
+            copy = copy_to(sib_out.at[k, r], sib_in.at[k, r], sb_s.at[k, n], sb_r.at[k, n], (sp, 2 * x + 1 - c))
+            copy.start()
+            crossing.append(copy)
+        return crossing
 
     def push(src, dst, k, e, d):
         copy = copy_to(src, dst, rs_s.at[k, e], rs_r.at[k, e], (sp, 2 * chip(d) + c))
         copy.start()
         sends.append(copy)
 
-    def pass_on(k, copy):
-        copy.wait()
-        outgoing[k, 2] = (own_part[k % 3, chip(2)] + sib_in[k, chip(2)].astype(F32)).astype(BF16)
-        local[chunk_rows(k), :] = own_part[k % 3, x] + sib_in[k, x].astype(F32)
+    def pass_on(k, crossing):
+        crossing[0].wait()
+        outgoing[k, 2] = (own_part[k % 3, 0] + sib_in[k, 0].astype(F32)).astype(BF16)
         for e, d in enumerate((1, -1)):
             half = pl.ds(share * e, share)
             push(outgoing.at[k, 2, half], relay.at[k, e], k, 2 + e, d)
+        for copy in crossing[1:]:
+            copy.wait()
+        local[chunk_rows(k), :] = own_part[k % 3, 3] + sib_in[k, 3].astype(F32)
 
     def push_near(k):
         for e, d in enumerate((1, -1)):
             copy_to(relay.at[k, e], relay.at[k, e], rs_s.at[k, 2 + e], rs_r.at[k, 2 + e], (sp, 2 * chip(d) + c)).wait_recv()
             half, rest = pl.ds(share * e, share), pl.ds(share * (1 - e), share)
-            total = own_part[k % 3, chip(d), half] + sib_in[k, chip(d), half].astype(F32)
+            total = own_part[k % 3, 1 + e, half] + sib_in[k, 1 + e, half].astype(F32)
             outgoing[k, e, half] = (total + relay[k, e].astype(F32)).astype(BF16)
-            total = own_part[k % 3, chip(d), rest] + sib_in[k, chip(d), rest].astype(F32)
+            total = own_part[k % 3, 1 + e, rest] + sib_in[k, 1 + e, rest].astype(F32)
             outgoing[k, e, rest] = total.astype(BF16)
-        for e, d in enumerate((1, -1)):
             push(outgoing.at[k, e], parts.at[e, chunk_rows(k)], k, e, d)
 
+    hidden(0)
     copy0 = compute(0)
+    hidden(1)
+    pass_on(0, copy0)
     copy1 = compute(1)
-    pass_on(0, copy0)
-    copy2 = compute(2)
+    hidden(2)
     pass_on(1, copy1)
     push_near(0)
-    copy3 = compute(3)
+    copy2 = compute(2)
+    hidden(3)
     pass_on(2, copy2)
     push_near(1)
+    copy3 = compute(3)
     pass_on(3, copy3)
-    push_near(2)
-    push_near(3)
+
     def parts_arrived(k):
         for e, d in enumerate((1, -1)):
             r = parts.at[e, chunk_rows(k)]
             copy_to(r, r, rs_s.at[k, e], rs_r.at[k, e], (sp, 2 * chip(d) + c)).wait_recv()
 
+    lane_at = lax.broadcasted_iota(jnp.int32, (128, 128), 1)
+    group = tiles // 2
+
+    def row_sums(g):
+        for t in range(group * g, group * g + group):
+            r = pl.ds(128 * t, 128)
+            y = local[r, :] + resid_scale * tok[r, my_cols].astype(F32)
+            for e in range(2):
+                y += parts[e, r, :].astype(F32)
+            local[r, :] = y
+            one = jnp.sum(y, axis=1, keepdims=True)
+            two = jnp.sum(y * y, axis=1, keepdims=True)
+            pair = jnp.where(lane_at == 0, one, jnp.where(lane_at == 1, two, 0.0))
+            at_lane = 128 * (t - group * g)
+            stat_out[g, :, at_lane : at_lane + 128] = jnp.transpose(pair)[0:2, :]
+        for d in range(1, n_tp):
+            copy = copy_to(stat_out.at[g], stat_in.at[g, d - 1], st_s.at[g, d - 1], st_r.at[g, d - 1], (sp, peer(d)))
+            copy.start()
+            sends.append(copy)
+
+    def stats_arrived(g):
+        for d in range(1, n_tp):
+            dst = stat_in.at[g, d - 1]
+            copy_to(dst, dst, st_s.at[g, d - 1], st_r.at[g, d - 1], (sp, peer(d))).wait_recv()
+
+    def all_sent():
+        for copy in sends + ring.sent + tg.sent:
+            copy.wait_send()
+
+    def second_norm(g):
+        stats = stat_out[g]
+        for d in range(1, n_tp):
+            stats += stat_in[g, d - 1]
+        mean = stats[0:1] * (1.0 / D)
+        scale = lax.rsqrt(stats[1:2] * (1.0 / D) - mean * mean + norm_eps)
+        lanes = pl.ds(128 * group * g, 128 * group)
+        rowq[0:1, lanes] = mean
+        rowq[1:2, lanes] = scale
+        for t in range(group * g, group * g + group):
+            r = pl.ds(128 * t, 128)
+            both = jnp.transpose(rowq[:, 128 * t : 128 * t + 128])
+            out[r, :] = ((local[r, :] - both[:, 0:1]) * both[:, 1:2] * last_gain[...].reshape(1, 256)).astype(BF16)
+
+    push_near(2)
     parts_arrived(0)
     parts_arrived(1)
+    row_sums(0)
+    push_near(3)
     parts_arrived(2)
     parts_arrived(3)
-
-    lane_at = lax.broadcasted_iota(jnp.int32, (128, 128), 1)
-    for t in range(tiles):
-        r = pl.ds(128 * t, 128)
-        y = local[r, :] + resid_scale * tok[r, my_cols].astype(F32)
-        for e in range(2):
-            y += parts[e, r, :].astype(F32)
-        local[r, :] = y
-        one = jnp.sum(y, axis=1, keepdims=True)
-        two = jnp.sum(y * y, axis=1, keepdims=True)
-        pair = jnp.where(lane_at == 0, one, jnp.where(lane_at == 1, two, 0.0))
-        stat_out[:, 128 * t : 128 * t + 128] = jnp.transpose(pair)[0:8, :]
-    for d in range(1, n_tp):
-        copy = copy_to(stat_out, stat_in.at[d - 1], st_s.at[d - 1], st_r.at[d - 1], (sp, peer(d)))
-        copy.start()
-        sends.append(copy)
-
-    def stats_arrived():
-        for d in range(1, n_tp):
-            copy_to(stat_in.at[d - 1], stat_in.at[d - 1], st_s.at[d - 1], st_r.at[d - 1], (sp, peer(d))).wait_recv()
-
-    def all_sent():
-        for copy in sends + ring.sent + wo.sent + tg.sent:
-            copy.wait_send()
-
-    stats_arrived()
-    stats = stat_out[...]
-    for d in range(1, n_tp):
-        stats += stat_in[d - 1]
-    mean = stats[0:1] * (1.0 / D)
-    scale = lax.rsqrt(stats[1:2] * (1.0 / D) - mean * mean + norm_eps)
-    rowq[0:1, :] = mean
-    rowq[1:2, :] = scale
-    for t in range(tiles):
-        r = pl.ds(128 * t, 128)
-        both = jnp.transpose(rowq[:, 128 * t : 128 * t + 128])
-        out[r, :] = ((local[r, :] - both[:, 0:1]) * both[:, 1:2] * last_gain[...].reshape(1, 256)).astype(BF16)
+    row_sums(1)
+    stats_arrived(0)
+    second_norm(0)
+    stats_arrived(1)
+    second_norm(1)
     all_sent()
 
 
@@ -658,9 +733,12 @@
     return pl.pallas_call(
         layer_kernel,
         out_shape=jax.ShapeDtypeStruct((rows, 256), BF16),
-        in_specs=[vmem] * 7 + [pl.BlockSpec(memory_space=pltpu.SMEM)] * 2 + [vmem] * 10,
+        in_specs=[pl.BlockSpec(memory_space=pl.ANY)] * 8 + [vmem] * 3 + [pl.BlockSpec(memory_space=pltpu.SMEM)] * 2
+        + [vmem] * 6,
         out_specs=vmem,
         scratch_shapes=[
+            pltpu.VMEM((rows, 256), BF16), pltpu.VMEM((rows, 128), BF16), pltpu.VMEM((rows, 128), BF16),
+            pltpu.VMEM((rows, 256), BF16), pltpu.VMEM((rows, 256), BF16), pltpu.VMEM((256, D), BF16),
             pltpu.VMEM((16, 256), BF16), pltpu.VMEM((16, 128), BF16), pltpu.VMEM((16, 128), BF16),
             pltpu.VMEM((16, 256), BF16), pltpu.VMEM((16, 128), BF16), pltpu.VMEM((16, 128), BF16),
             pltpu.VMEM((24, rows), F32), pltpu.VMEM((8, 256), F32),
@@ -676,24 +754,27 @@
             pltpu.VMEM((STATE + 16, 256), BF16), pltpu.VMEM((STATE + 16, 256), BF16),
             pltpu.VMEM((3, STATE + 16, 256), BF16), pltpu.VMEM((3, STATE + 16, 256), BF16),
             pltpu.VMEM((2, STATE, 256), F32),
-            pltpu.VMEM((D, 1024), BF16), pltpu.VMEM((D, 1024), BF16), pltpu.VMEM((D, D), BF16),
-            pltpu.VMEM((rows, 256), BF16), pltpu.VMEM((share, D), BF16), pltpu.VMEM((share, D), BF16),
+            pltpu.VMEM((D, 1024), BF16), pltpu.VMEM((D, 1024), BF16),
+            pltpu.VMEM((rows, 256), BF16), pltpu.VMEM((4, share, D), BF16), pltpu.VMEM((4, share, D), BF16),
+            pltpu.VMEM((4, share, D), F32), pltpu.VMEM((share, D), BF16), pltpu.VMEM((2, share, D), BF16),
+            pltpu.VMEM((2, share // 2, D), BF16), pltpu.VMEM((2, share, D), BF16), pltpu.VMEM((share, D), BF16),
             pltpu.VMEM((8, D), F32), pltpu.VMEM((share, D), F32), pltpu.VMEM((rows, D), BF16),
             pltpu.VMEM((2 * share, 1024), BF16),
             pltpu.VMEM((4, 4, 2 * share, 256), BF16), pltpu.VMEM((4, 4, 2 * share, 256), BF16),
             pltpu.VMEM((3, 4, 2 * share, 256), F32), pltpu.VMEM((4, 3, 2 * share, 256), BF16),
-            pltpu.VMEM((2, rows, 256), BF16), pltpu.VMEM((4, 2, share, 256), BF16), pltpu.VMEM((8, rows), F32), pltpu.VMEM((7, 8, rows), F32),
-            dma((6,)), dma((6,)), dma((10,)), dma((10,)),
+            pltpu.VMEM((2, rows, 256), BF16), pltpu.VMEM((4, 2, share, 256), BF16), pltpu.VMEM((2, 2, rows // 2), F32),
+            pltpu.VMEM((2, 7, 2, rows // 2), F32),
+            dma((8,)), dma((6,)), dma((6,)), dma((10,)), dma((10,)),
             dma((2,)), dma((2,)), dma((2,)), dma((2,)), dma((2, 4, 4)), dma((2, 4, 4)),
             dma((2, 4)), dma((2, 4)), dma((8, 2)), dma((8, 2)), dma((8, 2)), dma((8, 2)),
-            dma((8,)), dma((8,)), dma((8,)), dma((8,)), dma((3, 7)), dma((3, 7)),
-            dma((4,)), dma((4,)), dma((4, 4)), dma((4, 4)), dma((7,)), dma((7,)),
+            dma((10,)), dma((10,)), dma((8,)), dma((8,)), dma((2, 7)), dma((2, 7)),
+            dma((4, 2)), dma((4, 2)), dma((4, 4)), dma((4, 4)), dma((2, 7)), dma((2, 7)),
         ],
         compiler_params=pltpu.CompilerParams(
             collective_id=0, has_side_effects=True, vmem_limit_bytes=60 * 1024 * 1024),
         cost_estimate=pl.CostEstimate(flops=9_000_000_000, bytes_accessed=8_000_000, transcendentals=0),
         name="layer",
-    )(hv, em, rm, gate, step.T, sudden.T, docs, rate, bias, tv, te, tr, gain, up_in, down_in, out_weight, stream,
+    )(hv, em, rm, gate, stream, out_weight, up_in, down_in, step.T, sudden.T, docs, rate, bias, tv, te, tr, gain,
       first_gain, last_gain)
 
 

time: 113 us -> 107 us (0.947)
  Pallas kernels: 111 us -> 105 us
    pallas_call x1, Pallas kernels: 111 us -> 105 us  [per_device(): pl.pallas_call(layer_kernel, out_shape=jax.ShapeDtypeStruct((rows, 256),...]
where the time goes in v4:
time: 107 us
  Pallas kernels  105 us (98%)
  local copies, waits for them, and re-layouts  1.77 us (2%)
    pallas_call x1, Pallas kernels, per_device(): pl.pallas_call(layer_kernel, out_shape=jax.ShapeDtypeStruct((rows, 256),...  105 us

profile of v4, /device:TPU:1, one launch (start us, length us, event | category | flops | bytes accessed | tf_op | source)
XLA Modules:
  0.0 106.5 jit_solution(8066463496036686740)
XLA Ops:
  0.0 104.7 %layer.1 = bf16[768,256]{1,0:T(8,128)(2,1)} custom-call(bf16[768,256]{1,0:T(8,128)(2,1)} %hv_any.1, bf16[768,128]{1,0:T(8,128)(2,1)} %em_any.1, bf16[768,128]{1,0:T(8,128)(2,1)} %rm_any.1, bf16[768,256]{1,0:T(8,128)(2,1)} %gate_any.1, bf16[768,256]{1,0:T(8,128)(2,1)} %stream_any.1, bf16[256,2048]{1,0:T(8,128)(2,1)} %wout_any.1, bf16[64,1024]{1,0:T(8,128)(2,1)} %up_any.1, ...), custom_call_target="tpu_custom_call" | custom-call | flops 8999999488 | bytes 8000000 | tf_op jit(solution)/shard_map/layer/pallas_call | solution.py:733
  104.7 1.8 %copy.21 = bf16[768,256]{1,0:T(8,128)(2,1)} copy(bf16[768,256]{1,0:T(8,128)(2,1)} %layer.1) | data formatting | bytes 786432

commit v5 on v4

--- a/solution.py
+++ b/solution.py
@@ -42,10 +42,11 @@
 
 
 class WeightRing:
-    def __init__(self, up_in, down_in, up, down, sems, sp, tp):
+    def __init__(self, up_in, down_in, up, down, turned, sems, sp, tp):
         (self.uy_s, self.uy_r, self.uh_s, self.uh_r, self.uz_s, self.uz_r,
          self.dz_s, self.dz_r, self.dy_s, self.dy_r, self.dh_s, self.dh_r) = sems
         self.up_in, self.down_in, self.up, self.down, self.tp = up_in, down_in, up, down, tp
+        self.turned = turned
         self.y, self.z = lax.rem(sp, 4), sp // 4
         self.sent = []
 
@@ -147,14 +148,19 @@
             self.down_z(s, False)
         self.down_y(s)
 
-    def finish(self):
-        for s in range(5):
-            self.down_half(s, True)
+    def turn(self, s):
+        self.down_half(s, True)
+        for _, dz in self.planes(s):
+            plane = lax.rem(self.z + dz + 8, 8)
+            span = pl.ds(pl.multiple_of(plane * 256, 256), 256)
+            for j in range(4):
+                block = self.down[span, 256 * j : 256 * j + 256]
+                self.turned[256 * j : 256 * j + 256, span] = jnp.transpose(block)
 
 
 class TpGather:
-    def __init__(self, own, buf, size, send, recv, sp, tp):
-        self.own, self.buf, self.size, self.s, self.r, self.sp = own, buf, size, send, recv, sp
+    def __init__(self, buf, size, send, recv, sp, tp):
+        self.buf, self.size, self.s, self.r, self.sp = buf, size, send, recv, sp
         self.x, self.c = tp // 2, lax.rem(tp, 2)
         self.sent = []
 
@@ -174,18 +180,22 @@
         copy_to(dst, dst, self.s.at[k], self.r.at[k], (self.sp, self.slot(0, True))).wait_recv()
 
     def begin(self):
-        mine = self.rows(0, False)
-        self.send(self.own, mine, 0, 1, False)
-        self.send(self.own, mine, 1, -1, False)
-        self.send(self.own, mine, 2, 0, True)
+        for half in range(2):
+            for k, dx in ((0, 1), (1, -1)):
+                part = half if dx == 1 else 1 - half
+                mine = self.rows(0, False, part)
+                self.send(mine, mine, k + 8 * half, dx, False)
+        self.send(self.rows(0, False), self.rows(0, False), 2, 0, True)
 
     def relay(self):
         left, right = self.rows(-1, False), self.rows(1, False)
-        self.arrived(left, 0)
+        self.arrived(self.rows(-1, False, 0), 0)
         self.send(self.rows(-1, False, 0), self.rows(-1, False, 0), 3, 1, False)
+        self.arrived(self.rows(1, False, 1), 1)
+        self.send(self.rows(1, False, 1), self.rows(1, False, 1), 4, -1, False)
+        self.arrived(self.rows(-1, False, 1), 8)
         self.send(left, left, 5, 0, True)
-        self.arrived(right, 1)
-        self.send(self.rows(1, False, 1), self.rows(1, False, 1), 4, -1, False)
+        self.arrived(self.rows(1, False, 0), 9)
         self.send(right, right, 6, 0, True)
 
     def far(self):
@@ -204,7 +214,7 @@
     prev_v, prev_e, prev_r, next_v, next_e, next_r,
     per_token, gains_in, wide, rowq, cols, val, ent, ent32, rdo, weight, local,
     msg0, msg1, got0, got1, wmsg0, wmsg1, wgot0, wgot1, states,
-    up, down, norm_out, mix_sib, mix_got, mix_own, mix_far, mix_near, mix_relay, mix_in, stream_in, gains, first, tok, squares,
+    up, down, turned, norm_out, mix_sib, mix_got, mix_own, mix_far, mix_near, mix_relay, mix_in, stream_in, gains, first, tok, squares,
     sib_out, sib_in, own_part, outgoing, parts, relay, stat_out, stat_in,
     pull, halo_send, halo_recv, state_send, state_recv,
     uy_s, uy_r, uh_s, uh_r, uz_s, uz_r, dz_s, dz_r, dy_s, dy_r, dh_s, dh_r,
@@ -248,10 +258,10 @@
                                  at(step)))
     for copy in halos:
         copy.start()
-    ring = WeightRing(up_in, down_in, up, down,
+    ring = WeightRing(up_in, down_in, up, down, turned,
                       (uy_s, uy_r, uh_s, uh_r, uz_s, uz_r, dz_s, dz_r, dy_s, dy_r, dh_s, dh_r), sp, tp)
+    ring.up_step(0)
     ring.down_step(0)
-    ring.up_step(0)
 
     def my_lanes(ref, q):
         return ref.at[:, pl.ds(pl.multiple_of(q * 256, 256), 256)]
@@ -353,18 +363,10 @@
     wide[8 : 8 + rows, 0:256] = hv[...].astype(F32)
     wide[8 : 8 + rows, 256:384] = em[...].astype(F32)
     wide[8 : 8 + rows, 384:512] = rm[...].astype(F32)
-    for copy in halos:
-        copy.wait()
-    wide[0:8, 0:256] = prev_v[8:16, :].astype(F32)
-    wide[0:8, 256:384] = prev_e[8:16, :].astype(F32)
-    wide[0:8, 384:512] = prev_r[8:16, :].astype(F32)
-    wide[8 + rows : 16 + rows, 0:256] = next_v[0:8, :].astype(F32)
-    wide[8 + rows : 16 + rows, 256:384] = next_e[0:8, :].astype(F32)
-    wide[8 + rows : 16 + rows, 384:512] = next_r[0:8, :].astype(F32)
-
     whole_taps = tap_v[...].astype(F32)
     taps = (whole_taps[:, 0:128], whole_taps[:, 128:256], tap_e[...].astype(F32), tap_r[...].astype(F32))
-    for t in range(tiles):
+
+    def convolve(t):
         lo = 128 * t
         masks = [jnp.broadcast_to(cols[lo : lo + 128, CM + o : CM + o + 1], (128, 128)) for o in range(5)]
         for g in range(4):
@@ -383,14 +385,31 @@
             else:
                 rdo[lo : lo + 128, :] = act.astype(BF16)
 
-    state0 = jnp.zeros((STATE, 256), F32)
-    state1 = jnp.zeros((STATE, 256), F32)
-    for t in range(tiles):
+    def state_of(t, state0, state1):
         r = pl.ds(128 * t, 128)
         ent_t = jnp.transpose(ent32[r, :]).astype(BF16)
         v = val[r, :].astype(F32)
         state0 += jnp.dot(ent_t, (v * lanes_of(cols, r, W0)).astype(BF16), preferred_element_type=F32)
         state1 += jnp.dot(ent_t, (v * lanes_of(cols, r, W1)).astype(BF16), preferred_element_type=F32)
+        return state0, state1
+
+    state0 = state1 = jnp.zeros((STATE, 256), F32)
+    for t in range(1, tiles - 1):
+        convolve(t)
+        state0, state1 = state_of(t, state0, state1)
+    for copy in halos:
+        copy.wait()
+    wide[0:8, 0:256] = prev_v[8:16, :].astype(F32)
+    wide[0:8, 256:384] = prev_e[8:16, :].astype(F32)
+    wide[0:8, 384:512] = prev_r[8:16, :].astype(F32)
+    wide[8 + rows : 16 + rows, 0:256] = next_v[0:8, :].astype(F32)
+    wide[8 + rows : 16 + rows, 256:384] = next_e[0:8, :].astype(F32)
+    wide[8 + rows : 16 + rows, 384:512] = next_r[0:8, :].astype(F32)
+
+    for t in (0, tiles - 1):
+        convolve(t)
+        state0, state1 = state_of(t, state0, state1)
+
     def fill(msg, state, passing):
         msg[0:STATE, :] = state.astype(BF16)
         coarse = passing.astype(BF16)
@@ -475,10 +494,10 @@
     lax.fori_loop(tiles // 2 + 1, tiles, tile_step, 0)
     ring.down_step(2)
     ring.up_step(3)
-    ring.down_half(1, False)
     for copy in far_sends:
         copy.wait()
     ring.up_step(2)
+    ring.up_step(4)
     carried = []
     for m, wgot in enumerate((wgot0, wgot1)):
         once = passing_of(wgot.at[0])
@@ -531,8 +550,11 @@
         mix_far[...] = (mix_own[0] + mix_got[0].astype(F32)).astype(BF16)
         for e, d in enumerate((1, -1)):
             mix_push(mix_far.at[pl.ds(half_share * e, half_share)], mix_relay.at[e], 4 + e, d)
+        return [sends.pop(), sends.pop()]
 
     def mix_near_rest():
+        for copy in far_out:
+            copy.wait_send()
         for e, d in enumerate((1, -1)):
             crossing[1 + e].wait()
             rest = pl.ds(half_share * (1 - e), half_share)
@@ -557,16 +579,22 @@
 
     crossing = [project(0, 2)]
     crossing.append(project(1, 1))
-    mix_far_out()
+    far_out = mix_far_out()
     crossing.append(project(2, -1))
     crossing.append(project(3, 0))
+    ring.up_step(6)
+    ring.down_half(1, False)
+    ring.down_step(3)
     mix_near_rest()
-    ring.up_step(4)
+    ring.up_step(5)
+    ring.down_half(2, False)
     mix_near_last()
-    ring.down_step(3)
-    ring.up_step(5)
-    ring.up_step(6)
-    ring.down_half(2, False)
+    ring.turn(0)
+    ring.turn(1)
+    ring.up_step(7)
+    ring.up_step(9)
+    ring.down_step(4)
+    ring.down_half(3, False)
     exchanged(0, stream_in)
     exchanged(1, gains)
     mix_finish()
@@ -574,22 +602,20 @@
     mean = jnp.sum(f, axis=1, keepdims=True) * (1.0 / D)
     var = jnp.sum(f * f, axis=1, keepdims=True) * (1.0 / D) - mean * mean
     tok[mine, :] = ((f - mean) * lax.rsqrt(var + norm_eps) * gains[0:1, :]).astype(BF16)
-    tg = TpGather(tok.at[mine], tok, share, tk_s, tk_r, sp, tp)
+    tg = TpGather(tok, share, tk_s, tk_r, sp, tp)
     tg.begin()
-    ring.down_step(4)
-    ring.up_step(7)
     ring.up_step(8)
-    ring.down_half(3, False)
-    ring.up_step(9)
+    ring.up_step(10)
+    ring.turn(2)
+    ring.down_half(4, False)
     tg.relay()
-    ring.down_half(4, False)
-    ring.up_step(10)
     ring.up_step(11)
+    ring.up_step(12)
+    ring.turn(3)
+    ring.up_step(13)
     tg.far()
-    ring.up_step(12)
-    ring.up_step(13)
     ring.up_step(14)
-    ring.finish()
+    ring.turn(4)
     for k in (2, 5, 6, 7):
         tg.sibling(k)
 
@@ -607,8 +633,8 @@
         for n, d in enumerate((2, 1, -1, 0)):
             for other in (True, False):
                 q = 2 * chip(d) + (1 - c if other else c)
-                w = down[pl.ds(pl.multiple_of(q * 256, 256), 256), :]
-                part = lax.dot_general(sq, w, (((1,), (1,)), ((), ())), preferred_element_type=F32)
+                w = turned[:, pl.ds(pl.multiple_of(q * 256, 256), 256)]
+                part = jnp.dot(sq, w, preferred_element_type=F32)
                 if other:
                     sib_out[k, n] = part.astype(BF16)
                 else:
@@ -754,7 +780,7 @@
             pltpu.VMEM((STATE + 16, 256), BF16), pltpu.VMEM((STATE + 16, 256), BF16),
             pltpu.VMEM((3, STATE + 16, 256), BF16), pltpu.VMEM((3, STATE + 16, 256), BF16),
             pltpu.VMEM((2, STATE, 256), F32),
-            pltpu.VMEM((D, 1024), BF16), pltpu.VMEM((D, 1024), BF16),
+            pltpu.VMEM((D, 1024), BF16), pltpu.VMEM((D, 1024), BF16), pltpu.VMEM((1024, D), BF16),
             pltpu.VMEM((rows, 256), BF16), pltpu.VMEM((4, share, D), BF16), pltpu.VMEM((4, share, D), BF16),
             pltpu.VMEM((4, share, D), F32), pltpu.VMEM((share, D), BF16), pltpu.VMEM((2, share, D), BF16),
             pltpu.VMEM((2, share // 2, D), BF16), pltpu.VMEM((2, share, D), BF16), pltpu.VMEM((share, D), BF16),
@@ -767,7 +793,7 @@
             dma((8,)), dma((6,)), dma((6,)), dma((10,)), dma((10,)),
             dma((2,)), dma((2,)), dma((2,)), dma((2,)), dma((2, 4, 4)), dma((2, 4, 4)),
             dma((2, 4)), dma((2, 4)), dma((8, 2)), dma((8, 2)), dma((8, 2)), dma((8, 2)),
-            dma((10,)), dma((10,)), dma((8,)), dma((8,)), dma((2, 7)), dma((2, 7)),
+            dma((10,)), dma((10,)), dma((10,)), dma((10,)), dma((2, 7)), dma((2, 7)),
             dma((4, 2)), dma((4, 2)), dma((4, 4)), dma((4, 4)), dma((2, 7)), dma((2, 7)),
         ],
         compiler_params=pltpu.CompilerParams(

time: 107 us -> 104 us (0.972)
  Pallas kernels: 105 us -> 102 us
    pallas_call x1, Pallas kernels: 105 us -> 102 us  [per_device(): pl.pallas_call(layer_kernel, out_shape=jax.ShapeDtypeStruct((rows, 256),...]
where the time goes in v5:
time: 104 us
  Pallas kernels  102 us (98%)
  local copies, waits for them, and re-layouts  1.77 us (2%)
    pallas_call x1, Pallas kernels, per_device(): pl.pallas_call(layer_kernel, out_shape=jax.ShapeDtypeStruct((rows, 256),...  102 us

profile of v5, /device:TPU:1, one launch (start us, length us, event | category | flops | bytes accessed | tf_op | source)
XLA Modules:
  0.0 104.1 jit_solution(7944408614856028408)
XLA Ops:
  0.0 102.3 %layer.1 = bf16[768,256]{1,0:T(8,128)(2,1)} custom-call(bf16[768,256]{1,0:T(8,128)(2,1)} %hv_any.1, bf16[768,128]{1,0:T(8,128)(2,1)} %em_any.1, bf16[768,128]{1,0:T(8,128)(2,1)} %rm_any.1, bf16[768,256]{1,0:T(8,128)(2,1)} %gate_any.1, bf16[768,256]{1,0:T(8,128)(2,1)} %stream_any.1, bf16[256,2048]{1,0:T(8,128)(2,1)} %wout_any.1, bf16[64,1024]{1,0:T(8,128)(2,1)} %up_any.1, ...), custom_call_target="tpu_custom_call" | custom-call | flops 8999999488 | bytes 8000000 | tf_op jit(solution)/shard_map/layer/pallas_call | solution.py:759
  102.4 1.8 %copy.21 = bf16[768,256]{1,0:T(8,128)(2,1)} copy(bf16[768,256]{1,0:T(8,128)(2,1)} %layer.1) | data formatting | bytes 786432

commit v6 on v5

--- a/solution.py
+++ b/solution.py
@@ -11,6 +11,7 @@
 HEAD_DIM = 64
 STATE = 128
 REACH = 8
+CUT = 896
 MESH = pl.DeviceIdType.MESH
 norm_eps = 1e-05
 resid_scale = 1.4142135623730951
@@ -68,24 +69,25 @@
     def up_z(self, s, p, receive):
         for m, sign in enumerate((1, -1)):
             low, count = (32 * m, 32) if s == 3 else (0, 64)
+            r = self.rows(-sign * (s + 1 if receive else s), p, low, count)
+            piece = self.up.at[r, pl.ds(0, CUT)]
             if receive:
-                r = self.rows(-sign * (s + 1), p, low, count)
-                self.arrived(self.up.at[r], self.uz_s.at[m, s, p], self.uz_r.at[m, s, p])
+                self.arrived(piece, self.uz_s.at[m, s, p], self.uz_r.at[m, s, p])
             else:
-                r = self.rows(-sign * s, p, low, count)
-                src = self.up_in if s == 0 and p == 0 else self.up.at[r]
-                self.send(src, self.up.at[r], self.uz_s.at[m, s, p], self.uz_r.at[m, s, p], self.dev(sign, 0))
+                self.send(piece, piece, self.uz_s.at[m, s, p], self.uz_r.at[m, s, p], self.dev(sign, 0))
+
+    def both(self, r):
+        return enumerate((self.down.at[r], self.up.at[r, pl.ds(CUT, 1024 - CUT)]))
 
     def down_z(self, s, receive):
         for m, sign in enumerate((1, -1)):
             low, count = (32 * m, 32) if s == 3 else (0, 64)
-            if receive:
-                r = self.rows(-sign * (s + 1), 0, low, count)
-                self.arrived(self.down.at[r], self.dz_s.at[m, s], self.dz_r.at[m, s])
-            else:
-                r = self.rows(-sign * s, 0, low, count)
-                src = self.down_in if s == 0 else self.down.at[r]
-                self.send(src, self.down.at[r], self.dz_s.at[m, s], self.dz_r.at[m, s], self.dev(sign, 0))
+            r = self.rows(-sign * (s + 1 if receive else s), 0, low, count)
+            for w, piece in self.both(r):
+                if receive:
+                    self.arrived(piece, self.dz_s.at[w, m, s], self.dz_r.at[w, m, s])
+                else:
+                    self.send(piece, piece, self.dz_s.at[w, m, s], self.dz_r.at[w, m, s], self.dev(sign, 0))
 
     def planes(self, s):
         return [(0, 0)] if s == 0 else [(7, 4)] if s == 4 else [(2 * s - 1, -s), (2 * s, s)]
@@ -93,29 +95,28 @@
     def down_y(self, s):
         for k, dz in self.planes(s):
             for m, sign in enumerate((1, -1)):
-                r = self.rows(dz, 0)
-                src = self.down_in if s == 0 else self.down.at[r]
-                self.send(src, self.down.at[r], self.dy_s.at[k, m], self.dy_r.at[k, m], self.dev(0, sign))
+                for w, piece in self.both(self.rows(dz, 0)):
+                    self.send(piece, piece, self.dy_s.at[w, k, m], self.dy_r.at[w, k, m], self.dev(0, sign))
 
     def down_half(self, s, receive):
         for k, dz in self.planes(s):
             for m, sign in enumerate((1, -1)):
                 if receive:
-                    r = self.rows(dz, -2 * sign, 32 * m, 32)
-                    self.arrived(self.down.at[r], self.dh_s.at[k, m], self.dh_r.at[k, m])
+                    for w, piece in self.both(self.rows(dz, -2 * sign, 32 * m, 32)):
+                        self.arrived(piece, self.dh_s.at[w, k, m], self.dh_r.at[w, k, m])
                 else:
-                    self.arrived(self.down.at[self.rows(dz, -sign)], self.dy_s.at[k, m], self.dy_r.at[k, m])
-                    r = self.rows(dz, -sign, 32 * m, 32)
-                    self.send(self.down.at[r], self.down.at[r], self.dh_s.at[k, m], self.dh_r.at[k, m],
-                              self.dev(0, sign))
+                    for w, piece in self.both(self.rows(dz, -sign)):
+                        self.arrived(piece, self.dy_s.at[w, k, m], self.dy_r.at[w, k, m])
+                    for w, piece in self.both(self.rows(dz, -sign, 32 * m, 32)):
+                        self.send(piece, piece, self.dh_s.at[w, k, m], self.dh_r.at[w, k, m], self.dev(0, sign))
 
     def up_step(self, n):
         s, part = divmod(n, 3)
         if part == 0:
             if s == 0:
                 for m, sign in enumerate((1, -1)):
-                    self.send(self.up_in, self.up.at[self.rows(0, 0)], self.uy_s.at[m], self.uy_r.at[m],
-                              self.dev(0, sign))
+                    piece = self.up.at[self.rows(0, 0), pl.ds(0, CUT)]
+                    self.send(piece, piece, self.uy_s.at[m], self.uy_r.at[m], self.dev(0, sign))
             else:
                 self.up_z(s - 1, 0, True)
             if s < 4:
@@ -123,9 +124,9 @@
         elif part == 1:
             if s == 0:
                 for m, sign in enumerate((1, -1)):
-                    self.arrived(self.up.at[self.rows(0, -sign)], self.uy_s.at[m], self.uy_r.at[m])
-                    r = self.rows(0, -sign, 32 * m, 32)
-                    self.send(self.up.at[r], self.up.at[r], self.uh_s.at[m], self.uh_r.at[m], self.dev(0, sign))
+                    self.arrived(self.up.at[self.rows(0, -sign), pl.ds(0, CUT)], self.uy_s.at[m], self.uy_r.at[m])
+                    piece = self.up.at[self.rows(0, -sign, 32 * m, 32), pl.ds(0, CUT)]
+                    self.send(piece, piece, self.uh_s.at[m], self.uh_r.at[m], self.dev(0, sign))
             else:
                 self.up_z(s - 1, 1, True)
                 self.up_z(s - 1, 3, True)
@@ -135,7 +136,8 @@
         else:
             if s == 0:
                 for m, sign in enumerate((1, -1)):
-                    self.arrived(self.up.at[self.rows(0, -2 * sign, 32 * m, 32)], self.uh_s.at[m], self.uh_r.at[m])
+                    piece = self.up.at[self.rows(0, -2 * sign, 32 * m, 32), pl.ds(0, CUT)]
+                    self.arrived(piece, self.uh_s.at[m], self.uh_r.at[m])
             else:
                 self.up_z(s - 1, 2, True)
             if s < 4:
@@ -436,11 +438,9 @@
     for k, d in enumerate((1, 2)):
         for m, (msg, got, step) in enumerate(((msg0, got0, d), (msg1, got1, -d))):
             near_sends.append(copy_to(msg, got.at[k], state_send.at[2 * k + m], state_recv.at[2 * k + m], at(step)))
-    for copy in near_sends:
+    for copy in reversed(near_sends):
         copy.start()
-    ring.down_step(1)
     ring.up_step(1)
-    ring.down_half(0, False)
 
     low_lane = lax.broadcasted_iota(jnp.int32, (128, 128), 1) < HEAD_DIM
 
@@ -484,18 +484,18 @@
             window += got[k, 0:STATE, :].astype(F32) * (through[k] * source_mask[4 * m + k])
         fill(wmsg, window, through[2])
     far_sends = []
-    lax.fori_loop(tiles // 2, tiles // 2 + 1, tile_step, 0)
     for k, d in enumerate((1, 4, 7)):
         for m, (wmsg, wgot, step) in enumerate(((wmsg0, wgot0, d), (wmsg1, wgot1, -d))):
             n = 4 + 2 * k + m
             far_sends.append(copy_to(wmsg, wgot.at[k], state_send.at[n], state_recv.at[n], at(step)))
-    for copy in far_sends:
+    for copy in reversed(far_sends):
         copy.start()
-    lax.fori_loop(tiles // 2 + 1, tiles, tile_step, 0)
-    ring.down_step(2)
-    ring.up_step(3)
+    ring.down_step(1)
+    ring.down_half(0, False)
+    lax.fori_loop(tiles // 2, tiles, tile_step, 0)
     for copy in far_sends:
         copy.wait()
+    ring.up_step(3)
     ring.up_step(2)
     ring.up_step(4)
     carried = []
@@ -583,18 +583,17 @@
     crossing.append(project(2, -1))
     crossing.append(project(3, 0))
     ring.up_step(6)
+    ring.down_step(2)
     ring.down_half(1, False)
-    ring.down_step(3)
     mix_near_rest()
     ring.up_step(5)
+    mix_near_last()
+    ring.down_step(3)
     ring.down_half(2, False)
-    mix_near_last()
     ring.turn(0)
     ring.turn(1)
     ring.up_step(7)
     ring.up_step(9)
-    ring.down_step(4)
-    ring.down_half(3, False)
     exchanged(0, stream_in)
     exchanged(1, gains)
     mix_finish()
@@ -605,15 +604,17 @@
     tg = TpGather(tok, share, tk_s, tk_r, sp, tp)
     tg.begin()
     ring.up_step(8)
+    ring.down_step(4)
     ring.up_step(10)
+    ring.down_half(3, False)
     ring.turn(2)
-    ring.down_half(4, False)
     tg.relay()
     ring.up_step(11)
     ring.up_step(12)
-    ring.turn(3)
+    ring.down_half(4, False)
     ring.up_step(13)
     tg.far()
+    ring.turn(3)
     ring.up_step(14)
     ring.turn(4)
     for k in (2, 5, 6, 7):
@@ -657,19 +658,20 @@
         for e, d in enumerate((1, -1)):
             half = pl.ds(share * e, share)
             push(outgoing.at[k, 2, half], relay.at[k, e], k, 2 + e, d)
-        for copy in crossing[1:]:
-            copy.wait()
+        crossing[1].wait()
+        for e, d in enumerate((1, -1)):
+            rest = pl.ds(share * (1 - e), share)
+            outgoing[k, e, rest] = (own_part[k % 3, 1 + e, rest] + sib_in[k, 1 + e, rest].astype(F32)).astype(BF16)
+            push(outgoing.at[k, e, rest], parts.at[e, pl.ds(2 * share * k + share * (1 - e), share)], k, 4 + e, d)
         local[chunk_rows(k), :] = own_part[k % 3, 3] + sib_in[k, 3].astype(F32)
 
     def push_near(k):
         for e, d in enumerate((1, -1)):
             copy_to(relay.at[k, e], relay.at[k, e], rs_s.at[k, 2 + e], rs_r.at[k, 2 + e], (sp, 2 * chip(d) + c)).wait_recv()
-            half, rest = pl.ds(share * e, share), pl.ds(share * (1 - e), share)
+            half = pl.ds(share * e, share)
             total = own_part[k % 3, 1 + e, half] + sib_in[k, 1 + e, half].astype(F32)
             outgoing[k, e, half] = (total + relay[k, e].astype(F32)).astype(BF16)
-            total = own_part[k % 3, 1 + e, rest] + sib_in[k, 1 + e, rest].astype(F32)
-            outgoing[k, e, rest] = total.astype(BF16)
-            push(outgoing.at[k, e], parts.at[e, chunk_rows(k)], k, e, d)
+            push(outgoing.at[k, e, half], parts.at[e, pl.ds(2 * share * k + share * e, share)], k, e, d)
 
     hidden(0)
     copy0 = compute(0)
@@ -688,8 +690,9 @@
 
     def parts_arrived(k):
         for e, d in enumerate((1, -1)):
-            r = parts.at[e, chunk_rows(k)]
-            copy_to(r, r, rs_s.at[k, e], rs_r.at[k, e], (sp, 2 * chip(d) + c)).wait_recv()
+            for n, low in ((4 + e, share * (1 - e)), (e, share * e)):
+                r = parts.at[e, pl.ds(2 * share * k + low, share)]
+                copy_to(r, r, rs_s.at[k, n], rs_r.at[k, n], (sp, 2 * chip(d) + c)).wait_recv()
 
     lane_at = lax.broadcasted_iota(jnp.int32, (128, 128), 1)
     group = tiles // 2
@@ -716,8 +719,8 @@
             dst = stat_in.at[g, d - 1]
             copy_to(dst, dst, st_s.at[g, d - 1], st_r.at[g, d - 1], (sp, peer(d))).wait_recv()
 
-    def all_sent():
-        for copy in sends + ring.sent + tg.sent:
+    def all_sent(copies):
+        for copy in copies:
             copy.wait_send()
 
     def second_norm(g):
@@ -744,9 +747,10 @@
     row_sums(1)
     stats_arrived(0)
     second_norm(0)
+    all_sent(sends[: -2 * (n_tp - 1)] + ring.sent + tg.sent)
     stats_arrived(1)
     second_norm(1)
-    all_sent()
+    all_sent(sends[-2 * (n_tp - 1) :])
 
 
 def per_device(hv, em, rm, gate, step, sudden, document_index, rate, bias, tv, te, tr, gain,
@@ -792,9 +796,9 @@
             pltpu.VMEM((2, 7, 2, rows // 2), F32),
             dma((8,)), dma((6,)), dma((6,)), dma((10,)), dma((10,)),
             dma((2,)), dma((2,)), dma((2,)), dma((2,)), dma((2, 4, 4)), dma((2, 4, 4)),
-            dma((2, 4)), dma((2, 4)), dma((8, 2)), dma((8, 2)), dma((8, 2)), dma((8, 2)),
+            dma((2, 2, 4)), dma((2, 2, 4)), dma((2, 8, 2)), dma((2, 8, 2)), dma((2, 8, 2)), dma((2, 8, 2)),
             dma((10,)), dma((10,)), dma((10,)), dma((10,)), dma((2, 7)), dma((2, 7)),
-            dma((4, 2)), dma((4, 2)), dma((4, 4)), dma((4, 4)), dma((2, 7)), dma((2, 7)),
+            dma((4, 2)), dma((4, 2)), dma((4, 6)), dma((4, 6)), dma((2, 7)), dma((2, 7)),
         ],
         compiler_params=pltpu.CompilerParams(
             collective_id=0, has_side_effects=True, vmem_limit_bytes=60 * 1024 * 1024),

time: 104 us -> 103 us (level)
    pallas_call x1, Pallas kernels: 102 us -> 101 us  [per_device(): pl.pallas_call(layer_kernel, out_shape=jax.ShapeDtypeStruct((rows, 256),...]
where the time goes in v6:
time: 103 us
  Pallas kernels  101 us (98%)
  local copies, waits for them, and re-layouts  1.77 us (2%)
    pallas_call x1, Pallas kernels, per_device(): pl.pallas_call(layer_kernel, out_shape=jax.ShapeDtypeStruct((rows, 256),...  101 us

profile of v6, /device:TPU:1, one launch (start us, length us, event | category | flops | bytes accessed | tf_op | source)
XLA Modules:
  0.0 103.0 jit_solution(11817760069558983785)
XLA Ops:
  0.0 101.2 %layer.1 = bf16[768,256]{1,0:T(8,128)(2,1)} custom-call(bf16[768,256]{1,0:T(8,128)(2,1)} %hv_any.1, bf16[768,128]{1,0:T(8,128)(2,1)} %em_any.1, bf16[768,128]{1,0:T(8,128)(2,1)} %rm_any.1, bf16[768,256]{1,0:T(8,128)(2,1)} %gate_any.1, bf16[768,256]{1,0:T(8,128)(2,1)} %stream_any.1, bf16[256,2048]{1,0:T(8,128)(2,1)} %wout_any.1, bf16[64,1024]{1,0:T(8,128)(2,1)} %up_any.1, ...), custom_call_target="tpu_custom_call" | custom-call | flops 8999999488 | bytes 8000000 | tf_op jit(solution)/shard_map/layer/pallas_call | solution.py:763
  101.2 1.8 %copy.21 = bf16[768,256]{1,0:T(8,128)(2,1)} copy(bf16[768,256]{1,0:T(8,128)(2,1)} %layer.1) | data formatting | bytes 786432
